TPU v7x, 32 devices: a whole 2x2x4 slice. The times are simulated.
32 devices in a mesh: sp: 16 (over z, y, core), tp: 2 (over x).
Axes of the slice: x: 2, y: 2, z: 4, core: 2. Of those that a mesh axis runs over, the one named last changes fastest.
Arguments:
- latent: bfloat16 [4096, 2048], P(('sp', 'tp')), may hold values from -36 to 36
- condition: float32 [2048], replicated, may hold values from -16 to 16
- context: bfloat16 [256, 2048], P('sp'), may hold values from -6 to 6
- context_condition_vector: float32 [2048], replicated, may hold values from -6 to 6
- modulation_matrix: bfloat16 [3, 2048, 2048], P(None, 'sp', 'tp'), may hold values from -0.125 to 0.125
- query_matrix: bfloat16 [2048, 2048], P(None, 'tp'), may hold values from -0.125 to 0.125
- key_matrix: bfloat16 [2048, 2048], P(None, 'tp'), may hold values from -0.125 to 0.125
- value_matrix: bfloat16 [2048, 2048], P(None, 'tp'), may hold values from -0.125 to 0.125
- decay_input_weight: bfloat16 [2048, 32], replicated, may hold values from -0.125 to 0.125
- write_strength_weight: bfloat16 [2048, 32], replicated, may hold values from -0.125 to 0.125
- head_decay_rate: float32 [32], replicated, may hold values from 0 to 1, as said below
- write_strength_bias: float32 [32], replicated, may hold values from -20 to 0
- context_write_offset_bias: float32 [32], replicated, may hold values from 1.5 to 4.5
- log_spike_added: float32 [4096, 32], P('sp'), may hold values from -2 to 0, as said below
- head_norm_gain: float32 [128], replicated, may hold values from 0.1 to 1.9
- output_matrix: bfloat16 [2048, 2048], P('tp'), may hold values from -0.125 to 0.125
Outputs:
- mixed: bfloat16 [4096, 2048], P(('sp', 'tp'))
Inputs may be any that keep to these rules, and one draw needn't show every extreme that they name: `head_decay_rate`: positive. `log_spike_added`: no entry is positive.
All inputs are finite; a program needn't handle non-finite values.
Results may differ from a plain program's by a relative error of at most 0.018.
Values may be sent and summed in bfloat16 or wider, within the bound.
A program may use at most 128 MiB of HBM per device.

v0:
```python
import jax
import jax.numpy as jnp
from jax import lax
from jax.sharding import PartitionSpec as P

DK = 128
BLOCK = 64


EPSILON = 1e-06
TOP_PRECISION = lax.Precision.HIGHEST


def carried_in(value, axis, join, neutral, backward):
    count = lax.axis_size(axis)
    place = lax.axis_index(axis)
    ahead = count - 1 - place if backward else place
    gathered = jax.tree.map(
        lambda a, kind: lax.all_gather(a.astype(kind), axis), value, (jnp.bfloat16, jnp.bfloat16)
    )
    state = jax.tree.map(lambda a, e: jnp.zeros_like(a) + jnp.asarray(e, a.dtype), value, neutral)

    def one(lap, state):
        source = count - 1 - lap if backward else lap
        return join(
            state,
            jax.tree.map(
                lambda a, own: lax.dynamic_index_in_dim(a, source, 0, False).astype(own.dtype),
                gathered,
                value,
            ),
        )

    return lax.fori_loop(0, ahead, one, state)


def layer_norm(matrix):
    widened = matrix.astype(jnp.float32)
    centred = widened - jnp.mean(widened, axis=-1, keepdims=True)
    spread = jnp.mean(centred * centred, axis=-1, keepdims=True)
    return centred * lax.rsqrt(spread + EPSILON)


def modulate(matrix, shift_vec, scale_vec):
    return (layer_norm(matrix) * (1.0 + scale_vec) + shift_vec).astype(jnp.bfloat16)


def rounded(matrix):
    return lax.optimization_barrier(matrix.astype(jnp.bfloat16)).astype(jnp.float32)


def project(row_block, weight):
    return rounded(jnp.dot(row_block, weight, preferred_element_type=jnp.float32))


def unit_length(vectors):
    return vectors * lax.rsqrt(jnp.sum(vectors * vectors, axis=-1, keepdims=True) + EPSILON)


def orient(matrix, direction):
    return matrix if direction == 0 else jnp.flip(matrix, axis=0)


def to_blocks(matrix):
    block_count = matrix.shape[0] // BLOCK
    shaped = matrix.reshape((block_count, BLOCK) + matrix.shape[1:])
    return jnp.swapaxes(shaped, 1, 2)


def from_blocks(matrix):
    shaped = jnp.swapaxes(matrix, 1, 2)
    return shaped.reshape((shaped.shape[0] * shaped.shape[1],) + shaped.shape[2:])


def block_terms(key_rows, value_rows, logarithm_decay, strength):
    key_blocks = to_blocks(key_rows)
    value_blocks = to_blocks(value_rows)
    strength_blocks = to_blocks(strength)
    cumulative = jnp.cumsum(to_blocks(logarithm_decay), axis=-1)
    token_position = jnp.arange(BLOCK)
    inclusive = token_position[:, None] >= token_position[None, :]
    strictly = token_position[:, None] > token_position[None, :]
    spread_log = cumulative[..., :, None] - cumulative[..., None, :]
    decay_mat = jnp.where(inclusive, jnp.exp(jnp.where(inclusive, spread_log, 0.0)), 0.0)
    weighted = key_blocks * strength_blocks[..., None]
    lower_part = jnp.where(
        strictly,
        jnp.einsum("nhid,nhjd->nhij", weighted, key_blocks, precision=TOP_PRECISION) * decay_mat,
        0.0,
    )
    system = lower_part + jnp.eye(BLOCK, dtype=jnp.float32)
    right_side = jnp.concatenate(
        [value_blocks * strength_blocks[..., None], weighted * jnp.exp(cumulative)[..., None]],
        axis=-1,
    )
    solved = jax.scipy.linalg.solve_triangular(system, right_side, lower=True, unit_diagonal=True)
    value_width = value_blocks.shape[-1]
    final_log_value = cumulative[..., -1]
    decayed_keys = key_blocks * jnp.exp(final_log_value[..., None] - cumulative)[..., None]
    return (
        key_blocks,
        solved[..., :value_width],
        solved[..., value_width:],
        decayed_keys,
        final_log_value,
        cumulative,
        decay_mat,
    )


def advance(carried_state, state_update, correction_term, decayed_keys, final_log_value):
    fresh_values = state_update - jnp.einsum(
        "xui,xij->xuj", correction_term, carried_state, precision=TOP_PRECISION
    )
    following_rows = carried_state * jnp.exp(final_log_value)[:, None, None] + jnp.einsum(
        "fga,fgo->fao", decayed_keys, fresh_values, precision=TOP_PRECISION
    )
    return (fresh_values, following_rows)


def final_state(key_rows, value_rows, logarithm_decay, strength, start_state):
    block_parts = block_terms(key_rows, value_rows, logarithm_decay, strength)

    def final_block_step(carried_state, inputs):
        fresh_values, following_rows = advance(carried_state, *inputs)
        return (following_rows, None)

    carried_state, _ = lax.scan(final_block_step, start_state, block_parts[1:5])
    return carried_state


def read_out(query_rows, block_parts, start_state):
    (
        key_blocks,
        state_update,
        correction_term,
        decayed_keys,
        final_log_value,
        cumulative,
        decay_mat,
    ) = block_parts
    query_blocks = to_blocks(query_rows)
    query_decayed = query_blocks * jnp.exp(cumulative)[..., None]
    token_position = jnp.arange(BLOCK)
    inclusive = token_position[:, None] >= token_position[None, :]
    scores = jnp.where(
        inclusive,
        jnp.einsum("nhid,nhjd->nhij", query_blocks, key_blocks, precision=TOP_PRECISION)
        * decay_mat,
        0.0,
    )

    def read_block_step(carried_state, inputs):
        piece_update, piece_fix, piece_keys, piece_log, segment_query, piece_score = inputs
        fresh_values, following_rows = advance(
            carried_state, piece_update, piece_fix, piece_keys, piece_log
        )
        result_output = jnp.einsum(
            "xui,xij->xuj", segment_query, carried_state, precision=TOP_PRECISION
        )
        result_output = result_output + jnp.einsum(
            "hij,hjv->hiv", piece_score, fresh_values, precision=TOP_PRECISION
        )
        return (following_rows, result_output)

    _, result_output = lax.scan(
        read_block_step,
        start_state,
        (state_update, correction_term, decayed_keys, final_log_value, query_decayed, scores),
    )
    return from_blocks(result_output)


def compose(preceding_map, subsequent_map):
    linear = jnp.einsum(
        "hkj,hjl->hkl", subsequent_map[0], preceding_map[0], precision=TOP_PRECISION
    )
    offset = (
        jnp.einsum("nmy,nyx->nmx", subsequent_map[0], preceding_map[1], precision=TOP_PRECISION)
        + subsequent_map[1]
    )
    return (linear, offset)


def device_map(block_parts, identity_mat):
    (
        key_blocks,
        state_update,
        correction_term,
        decayed_keys,
        final_log_value,
        cumulative,
        decay_mat,
    ) = block_parts
    linear = jnp.exp(final_log_value)[..., None, None] * identity_mat
    linear = linear - jnp.einsum(
        "nhck,nhcj->nhkj", decayed_keys, correction_term, precision=TOP_PRECISION
    )
    offset = jnp.einsum("nhck,nhcv->nhkv", decayed_keys, state_update, precision=TOP_PRECISION)

    def device_block_step(carried_state, inputs):
        return (compose(carried_state, inputs), None)

    result_output, _ = lax.scan(
        device_block_step, (identity_mat, jnp.zeros_like(identity_mat)), (linear, offset)
    )
    return result_output


def per_device(
    latent,
    condition,
    context,
    context_condition_vector,
    modulation_matrix,
    query_matrix,
    key_matrix,
    value_matrix,
    decay_input_weight,
    write_strength_weight,
    head_decay_rate,
    write_strength_bias,
    context_write_offset_bias,
    log_spike_added,
    head_norm_gain,
    output_matrix,
):
    sp_index = lax.axis_index("sp")
    tp_index = lax.axis_index("tp")
    rows_part = modulation_matrix.shape[1]
    mod_float = modulation_matrix.astype(jnp.float32)
    latent_signal = lax.dynamic_slice_in_dim(
        jax.nn.silu(condition), sp_index * rows_part, rows_part
    )
    context_signal = lax.dynamic_slice_in_dim(
        jax.nn.silu(context_condition_vector), sp_index * rows_part, rows_part
    )
    latent_part = jnp.einsum("i,rij->rj", latent_signal, mod_float, precision=TOP_PRECISION)
    context_part = jnp.einsum("i,rij->rj", context_signal, mod_float[:2], precision=TOP_PRECISION)
    latent_sum, context_sum = lax.psum((latent_part, context_part), "sp")
    latent_factors, context_factors = (
        lax.all_gather(latent_sum, "tp", axis=1, tiled=True),
        lax.all_gather(context_sum, "tp", axis=1, tiled=True),
    )
    hidden = lax.all_gather(
        modulate(latent, latent_factors[0], latent_factors[1]), "tp", axis=0, tiled=True
    )
    length_total = hidden.shape[0]
    resident_heads = query_matrix.shape[1] // DK
    leading_column = tp_index * 2 * resident_heads
    rate_cols = lax.dynamic_slice_in_dim(decay_input_weight, leading_column, 2 * resident_heads, 1)
    write_cols = lax.dynamic_slice_in_dim(
        write_strength_weight, leading_column, 2 * resident_heads, 1
    )
    decay_rates = lax.dynamic_slice_in_dim(
        head_decay_rate, leading_column, 2 * resident_heads
    ).reshape(resident_heads, 2)
    write_biases = lax.dynamic_slice_in_dim(
        write_strength_bias, leading_column, 2 * resident_heads
    ).reshape(resident_heads, 2)
    context_biases = write_biases + lax.dynamic_slice_in_dim(
        context_write_offset_bias, leading_column, 2 * resident_heads
    ).reshape(resident_heads, 2)
    spike_values = lax.dynamic_slice_in_dim(
        log_spike_added, leading_column, 2 * resident_heads, 1
    ).reshape(length_total, resident_heads, 2)
    queries = project(hidden, query_matrix).reshape(length_total, resident_heads, DK)
    latent_keys = unit_length(project(hidden, key_matrix).reshape(length_total, resident_heads, DK))
    latent_values = project(hidden, value_matrix).reshape(length_total, resident_heads, DK)
    logarithm_decay = (
        -decay_rates
        * jax.nn.softplus(project(hidden, rate_cols).reshape(length_total, resident_heads, 2))
        + spike_values
    )
    strength = jax.nn.sigmoid(
        project(hidden, write_cols).reshape(length_total, resident_heads, 2) + write_biases
    )
    context_own = modulate(context, context_factors[0], context_factors[1])
    key_part = jnp.dot(context_own, key_matrix, preferred_element_type=jnp.float32).astype(
        jnp.bfloat16
    )
    value_part = jnp.dot(context_own, value_matrix, preferred_element_type=jnp.float32).astype(
        jnp.bfloat16
    )
    rate_part = jnp.dot(context_own, rate_cols, preferred_element_type=jnp.float32).astype(
        jnp.bfloat16
    )
    write_part = jnp.dot(context_own, write_cols, preferred_element_type=jnp.float32).astype(
        jnp.bfloat16
    )
    paired = jnp.concatenate([key_part, value_part], axis=1)
    gate_inputs = jnp.concatenate([rate_part, write_part], axis=1)
    paired_all, gates_all = (
        lax.all_gather(paired, "sp", axis=0, tiled=True),
        lax.all_gather(gate_inputs, "sp", axis=0, tiled=True),
    )
    key_width = key_matrix.shape[1]
    context_key_raw = paired_all[:, :key_width].astype(jnp.float32)
    context_value_raw = paired_all[:, key_width:].astype(jnp.float32)
    context_rate_raw = gates_all[:, : 2 * resident_heads].astype(jnp.float32)
    context_write_raw = gates_all[:, 2 * resident_heads :].astype(jnp.float32)
    context_length = context_key_raw.shape[0]
    context_keys = unit_length(context_key_raw.reshape(context_length, resident_heads, DK))
    context_values = context_value_raw.reshape(context_length, resident_heads, DK)
    context_decay = -decay_rates * jax.nn.softplus(
        context_rate_raw.reshape(context_length, resident_heads, 2)
    )
    context_strength = jax.nn.sigmoid(
        context_write_raw.reshape(context_length, resident_heads, 2) + context_biases
    )
    identity_mat = jnp.broadcast_to(jnp.eye(DK, dtype=jnp.float32), (resident_heads, DK, DK))
    zero_state = jnp.zeros((resident_heads, DK, DK), jnp.float32)
    summed = jnp.zeros((length_total, resident_heads, DK), jnp.float32)
    for direction in range(2):
        carried_state = final_state(
            orient(context_keys, direction),
            orient(context_values, direction),
            orient(context_decay[..., direction], direction),
            orient(context_strength[..., direction], direction),
            zero_state,
        )
        block_parts = block_terms(
            orient(latent_keys, direction),
            orient(latent_values, direction),
            orient(logarithm_decay[..., direction], direction),
            orient(strength[..., direction], direction),
        )
        map_linear, map_offset = device_map(block_parts, identity_mat)
        if direction == 0:
            context_prefix = carried_in(
                (map_linear, map_offset), "sp", compose, (identity_mat, zero_state), False
            )
        else:
            context_prefix = carried_in(
                (map_linear, map_offset), "sp", compose, (identity_mat, zero_state), True
            )
        initial_state = (
            jnp.einsum("nmy,nyx->nmx", context_prefix[0], carried_state, precision=TOP_PRECISION)
            + context_prefix[1]
        )
        summed = summed + orient(
            read_out(orient(queries, direction), block_parts, initial_state), direction
        )
    normed = (
        summed
        * lax.rsqrt(jnp.mean(summed * summed, axis=-1, keepdims=True) + EPSILON)
        * head_norm_gain
    )
    normed = normed.astype(jnp.bfloat16).reshape(length_total, resident_heads * DK)
    branch = lax.psum_scatter(
        jnp.dot(normed, output_matrix, preferred_element_type=jnp.float32).astype(jnp.bfloat16),
        "tp",
        scatter_dimension=0,
        tiled=True,
    ).astype(jnp.float32)
    return (latent.astype(jnp.float32) + latent_factors[2] * branch).astype(jnp.bfloat16)


def solution(mesh):
    in_specs = (
        P(("sp", "tp"), None),
        P(),
        P("sp", None),
        P(),
        P(None, "sp", "tp"),
        P(None, "tp"),
        P(None, "tp"),
        P(None, "tp"),
        P(),
        P(),
        P(),
        P(),
        P(),
        P("sp", None),
        P(),
        P("tp", None),
    )
    out_specs = P(("sp", "tp"), None)
    return jax.shard_map(
        per_device, mesh=mesh, in_specs=in_specs, out_specs=out_specs, check_vma=False
    )
```

profile of v0, /device:TPU:0, one launch (start us, length us, event | category | flops | bytes accessed | tf_op | source)
XLA Modules:
  0.0 1045.3 jit_solution(10574678594592969745)
XLA Ops:
  9.7 63.0 %all-reduce = (f32[3,1024]{1,0:T(4,128)S(1)}, f32[2,1024]{1,0:T(2,128)S(1)}) all-reduce(f32[3,1024]{1,0:T(4,128)S(1)} %bitcast.471, f32[2,1024]{1,0:T(2,128)S(1)} %bitcast.481), channel_id=1, replica_groups=mesh['sp'=16,'tp'=2] {'sp'}, use_global_device_ids=true, to_apply=%region_0.1 | all-reduce | flops 5120 | bytes 40960 | tf_op jit(solution)/shard_map/psum | solution.py:240
  72.7 4.4 all_gather.39
  79.9 4.4 all_gather.45
  84.7 3.1 convolution_convert_fusion.4
  91.5 17.3 %all_gather.46 = bf16[256,32]{1,0:T(8,128)(2,1)S(1)} all-gather(bf16[16,32]{1,0:T(8,128)(2,1)S(1)} %pad_maximum_fusion.1), channel_id=1, replica_groups=mesh['sp'=16,'tp'=2] {'sp'}, dimensions={0}, use_global_device_ids=true | all-gather | bytes 17408 | tf_op jit(solution)/shard_map/all_gather | solution.py:295
  113.6 3.8 convolution_convert_fusion.3
  119.8 3.6 convolution_convert_fusion.1
  126.6 3.7 fusion.187
  130.3 158.7 %custom-call.10 = f32[4,8,1,64,64]{3,4,2,1,0:T(8,128)} custom-call(f32[4,8,1,64,64]{4,3,2,1,0:T(8,128)} %fusion.187), custom_call_target="InvertDiagBlocksLowerTriangular" | custom-call | tf_op jit(solution)/shard_map/jit(_solve_triangular)/vmap(vmap())/triangular_solve | solution.py:96
  293.3 4.9 fusion.265
  298.2 3.7 multiply_subtract_fusion.1
  302.0 14.3 %while.102 = (s32[]{:T(128)}, f32[8,128,128]{2,1,0:T(8,128)S(1)}, f32[8,128,128]{2,1,0:T(8,128)}, f32[4,8,128,128]{3,2,1,0:T(8,128)S(1)}, f32[4,8,128,128]{3,2,1,0:T(8,128)}, /*index=5*/s32[]{:T(128)}, s32[]{:T(128)}) while((s32[]{:T(128)}, f32[8,128,128]{2,1,0:T(8,128)S(1)}, f32[8,128,128]{2,1,0:T(8,128)}, ...), condition=%wide.region_6.8_spmd.clone, body=%wide.region_5.7_spmd.clone.sunk | while | flops 402915328 | bytes 7865982 | solution.py:204
  325.7 3.0 fusion.157
  328.7 158.7 %custom-call.12 = f32[4,8,1,64,64]{3,4,2,1,0:T(8,128)} custom-call(f32[4,8,1,64,64]{4,3,2,1,0:T(8,128)} %fusion.157), custom_call_target="InvertDiagBlocksLowerTriangular" | custom-call | tf_op jit(solution)/shard_map/jit(_solve_triangular)/vmap(vmap())/triangular_solve | solution.py:96
  491.3 4.9 fusion.262
  496.2 3.7 multiply_subtract_fusion
  499.9 14.5 %while.104 = (s32[]{:T(128)}, f32[8,128,128]{2,1,0:T(8,128)S(1)}, f32[8,128,128]{2,1,0:T(8,128)}, f32[4,8,128,128]{3,2,1,0:T(8,128)S(1)}, f32[4,8,128,128]{3,2,1,0:T(8,128)}, /*index=5*/s32[]{:T(128)}, s32[]{:T(128)}) while((s32[]{:T(128)}, f32[8,128,128]{2,1,0:T(8,128)S(1)}, f32[8,128,128]{2,1,0:T(8,128)}, ...), condition=%wide.region_20.22_spmd.clone, body=%wide.region_19.21_spmd.clone.sunk | while | flops 402915328 | bytes 7865982 | solution.py:204
  501.2 2.5 convolution_add_fusion.26
  504.8 2.5 convolution_add_fusion.26
  521.4 3.7 fusion.129
  529.7 3.0 fusion.128
  537.6 4.7 fusion.172
  542.3 158.7 %custom-call.11 = f32[4,8,1,64,64]{3,4,2,1,0:T(8,128)} custom-call(f32[4,8,1,64,64]{4,3,2,1,0:T(8,128)} %fusion.172), custom_call_target="InvertDiagBlocksLowerTriangular" | custom-call | tf_op jit(solution)/shard_map/jit(_solve_triangular)/vmap(vmap())/triangular_solve | solution.py:96
  706.7 14.9 %while.103 = (s32[]{:T(128)}, f32[8,128,128]{2,1,0:T(8,128)S(1)}, f32[4,8]{1,0:T(4,128)S(1)}, f32[4,8,64,128]{3,2,1,0:T(8,128)}, f32[4,8,64,128]{3,2,1,0:T(8,128...) while((s32[]{:T(128)}, f32[8,128,128]{2,1,0:T(8,128)S(1)}, f32[4,8]{1,0:T(4,128)S(1)}, ...), condition=%wide.region_15.17_spmd.clone, body=%wide.region_14.16_spmd.clone.sunk | while | flops 201916416 | bytes 2885327 | solution.py:128
  725.5 3.0 fusion.142
  728.4 158.7 %custom-call.13 = f32[4,8,1,64,64]{3,4,2,1,0:T(8,128)} custom-call(f32[4,8,1,64,64]{4,3,2,1,0:T(8,128)} %fusion.142), custom_call_target="InvertDiagBlocksLowerTriangular" | custom-call | tf_op jit(solution)/shard_map/jit(_solve_triangular)/vmap(vmap())/triangular_solve | solution.py:96
  892.5 11.0 %while.105 = (s32[]{:T(128)}, f32[8,128,128]{2,1,0:T(8,128)S(1)}, f32[4,8]{1,0:T(4,128)S(1)}, f32[4,8,64,128]{3,2,1,0:T(8,128)S(1)}, f32[4,8,64,128]{3,2,1,0:T(8...) while((s32[]{:T(128)}, f32[8,128,128]{2,1,0:T(8,128)S(1)}, ...), condition=%wide.region_25.27_spmd.clone, body=%wide.region_24.26_spmd.clone.sunk | while | flops 201916416 | bytes 2885807 | solution.py:128
  905.4 32.4 %while.99 = (s32[]{:T(128)}, f32[8,128,128]{2,1,0:T(8,128)S(1)}, f32[4,8,64,128]{3,1,2,0:T(8,128)}, f32[4,8]{1,0:T(4,128)}, f32[4,8,64,128]{3,2,1,0:T(8,128)}, /...) while((s32[]{:T(128)}, f32[8,128,128]{2,1,0:T(8,128)S(1)}, ...), condition=%wide.region_17.19_spmd, body=%wide.region_16.18_spmd.sunk | while | flops 352714752 | bytes 5506273 | solution.py:166
  937.8 43.8 %while.100 = (s32[]{:T(128)}, f32[8,128,128]{2,1,0:T(8,128)S(1)}, f32[8,128,128]{2,1,0:T(8,128)S(1)}, s32[]{:T(128)}, bf16[16,8,128,128]{3,2,1,0:T(8,128)(2,1)},...) while((s32[]{:T(128)}, f32[8,128,128]{2,1,0:T(8,128)S(1)}, ...), condition=%wide.region_22.24_spmd, body=%wide.region_21.23_spmd.sunk | while | flops 402915328 | bytes 4981919 | solution.py:34
  982.4 27.6 %while.101 = (s32[]{:T(128)}, f32[8,128,128]{2,1,0:T(8,128)S(1)}, f32[4,8,64,128]{3,1,2,0:T(8,128)S(1)}, f32[4,8]{1,0:T(4,128)S(1)}, f32[4,8,64,128]{3,2,1,0:T(8...) while((s32[]{:T(128)}, f32[8,128,128]{2,1,0:T(8,128)S(1)}, ...), condition=%wide.region_27.29_spmd, body=%wide.region_26.28_spmd.sunk | while | flops 352714752 | bytes 5506273 | solution.py:166
  1012.2 4.5 convolution_convert_fusion
  1016.8 19.2 %reduce-scatter.2.cloned.1.call-done = bf16[128,2048]{1,0:T(8,128)(2,1)} async-done(((bf16[256,2048]{1,0:T(8,128)(2,1)}), bf16[128,2048]{1,0:T(8,128)(2,1)}) %reduce-scatter.2.cloned.1.call-update) | async-done | bytes 524304 | tf_op jit(solution)/shard_map/reduce_scatter | solution.py:350
  (459 shorter events, 226.7 us)
Async XLA Ops:
  6.5 84.7 %copy-start = (bf16[2048,32]{0,1:T(8,128)(2,1)S(1)}, bf16[2048,32]{0,1:T(8,128)(2,1)}, u32[]{:S(2)}) copy-start(bf16[2048,32]{0,1:T(8,128)(2,1)} %param.42) | copy-start | bytes 393220
  6.5 71.8 %copy-start.20 = (bf16[128,2048]{1,0:T(8,128)(2,1)S(1)}, bf16[128,2048]{1,0:T(8,128)(2,1)}, u32[]{:S(2)}) copy-start(bf16[128,2048]{1,0:T(8,128)(2,1)} %param.34) | copy-start | bytes 1572868
  6.5 103.5 %all-gather.11.cloned.1.call-start = ((), (), s32[]{:S(2)}) async-start(), calls=%async_computation.1 | async-start | bytes 1572864 | tf_op jit(solution)/shard_map/all_gather | solution.py:245
  6.5 77.8 %copy-start.28 = (bf16[16,2048]{1,0:T(8,128)(2,1)S(1)}, bf16[16,2048]{1,0:T(8,128)(2,1)}, u32[]{:S(2)}) copy-start(bf16[16,2048]{1,0:T(8,128)(2,1)} %param.36) | copy-start | bytes 196612
  79.9 452.9 %all-gather.13.cloned.1.call-start = ((), (), s32[]{:S(2)}) async-start(), calls=%async_computation.2 | async-start | bytes 1114112 | tf_op jit(solution)/shard_map/all_gather | solution.py:294
  84.7 3.6 copy-start.24
  88.3 20.7 %copy-start.52 = (f32[32]{0:T(128)S(1)}, f32[32]{0:T(128)}, u32[]{:S(2)}) copy-start(f32[32]{0:T(128)} %param.44) | copy-start | bytes 388
  88.3 20.9 %copy-start.46 = (f32[256,32]{0,1:T(8,128)S(1)}, f32[256,32]{0,1:T(8,128)}, u32[]{:S(2)}) copy-start(f32[256,32]{0,1:T(8,128)} %param.47) | copy-start | bytes 98308
  88.3 20.9 %copy-start.53 = (f32[32]{0:T(128)S(1)}, f32[32]{0:T(128)}, u32[]{:S(2)}) copy-start(f32[32]{0:T(128)} %param.45) | copy-start | bytes 388
  89.6 813.9 %all-gather.15.cloned.1.call-start = ((), (), s32[]{:S(2)}) async-start(), calls=%async_computation.4 | async-start | bytes 4456448 | tf_op jit(solution)/shard_map/all_gather | solution.py:19
  113.5 3.9 copy-start.42
  118.6 170.4 %copy-start.11 = (f32[32,8,8,128]{3,2,1,0:T(8,128)}, f32[32,8,8,128]{3,2,1,0:T(8,128)S(1)}, u32[]{:S(2)}) copy-start(f32[32,8,8,128]{3,2,1,0:T(8,128)S(1)} %copy.211) | copy-start | bytes 3145732
  119.8 4.7 copy-start.25
  124.5 164.5 %copy-start.17 = (f32[32,8,8,128]{3,2,1,0:T(8,128)}, f32[32,8,8,128]{3,2,1,0:T(8,128)S(1)}, u32[]{:S(2)}) copy-start(f32[32,8,8,128]{3,2,1,0:T(8,128)S(1)} %copy.217) | copy-start | bytes 3145732
  126.2 162.8 %copy-start.19 = (f32[32,8,8,128]{3,2,1,0:T(8,128)}, f32[32,8,8,128]{3,2,1,0:T(8,128)S(1)}, u32[]{:S(2)}) copy-start(f32[32,8,8,128]{3,2,1,0:T(8,128)S(1)} %copy.213) | copy-start | bytes 3145732
  291.3 6.9 copy-start.3
  293.3 4.9 copy-start.7
  317.1 586.5 %all-gather.17.cloned.1.call-start = ((), (), s32[]{:S(2)}) async-start(), calls=%async_computation.5 | async-start | bytes 4456448 | tf_op jit(solution)/shard_map/all_gather | solution.py:19
  319.0 618.8 %all-gather.19.cloned.1.call-start = ((), (), s32[]{:S(2)}) async-start(), calls=%async_computation.6 | async-start | bytes 4456448 | tf_op jit(solution)/shard_map/all_gather | solution.py:19
  321.8 165.6 %copy-start.13 = (f32[256,8,128]{2,1,0:T(8,128)}, f32[256,8,128]{2,1,0:T(8,128)S(1)}, u32[]{:S(2)}) copy-start(f32[256,8,128]{2,1,0:T(8,128)S(1)} %rev.33) | copy-start | bytes 3145732
  322.9 164.6 %copy-start.15 = (f32[256,8,128]{2,1,0:T(8,128)}, f32[256,8,128]{2,1,0:T(8,128)S(1)}, u32[]{:S(2)}) copy-start(f32[256,8,128]{2,1,0:T(8,128)S(1)} %rev.40) | copy-start | bytes 3145732
  489.2 6.9 copy-start.2
  491.3 4.9 copy-start.9
  499.9 15.5 %copy-start.54 = (f32[32]{0:T(128)S(1)}, f32[32]{0:T(128)}, u32[]{:S(2)}) copy-start(f32[32]{0:T(128)} %param.46) | copy-start | bytes 388
  514.5 3.6 copy-start.6
  515.3 422.5 %all-gather.21.cloned.1.call-start = ((), (), s32[]{:S(2)}) async-start(), calls=%async_computation.7 | async-start | bytes 4456448 | tf_op jit(solution)/shard_map/all_gather | solution.py:19
  518.9 6.2 copy-start.8
  532.7 503.3 %reduce-scatter.2.cloned.1.call-start = ((), (), s32[]{:S(2)}) async-start(), calls=%async_computation.3 | async-start | bytes 1572864 | tf_op jit(solution)/shard_map/reduce_scatter | solution.py:350
  724.2 4.2 copy-start.22
  725.5 161.7 %copy-start.23 = (f32[256,8,128]{2,1,0:T(8,128)S(1)}, f32[256,8,128]{2,1,0:T(8,128)}, u32[]{:S(2)}) copy-start(f32[256,8,128]{2,1,0:T(8,128)} %rev.39) | copy-start | bytes 3145732
  1012.2 23.8 %copy-start.21 = (bf16[128,2048]{1,0:T(8,128)(2,1)S(1)}, bf16[128,2048]{1,0:T(8,128)(2,1)}, u32[]{:S(2)}) copy-start(bf16[128,2048]{1,0:T(8,128)(2,1)} %param.34) | copy-start | bytes 1572868
  1012.2 25.8 %copy-start.1 = (bf16[2048,32]{0,1:T(8,128)(2,1)S(1)}, bf16[2048,32]{0,1:T(8,128)(2,1)}, u32[]{:S(2)}) copy-start(bf16[2048,32]{0,1:T(8,128)(2,1)} %param.42) | copy-start | bytes 393220
  (36 other events, 66.3 us)
Sparse Core Ops, SparseCore 0:
  80.0 18.5 all-gather.10
  100.7 38.0 all-gather.12
  317.2 50.0 all-gather.14
  369.3 49.7 all-gather.16
  515.4 49.8 all-gather.18
  567.3 49.2 all-gather.20
  1016.9 19.0 reduce-scatter.1
where the time goes:
time: 1060 us; the launch traced here: 1050 us
  other arithmetic  667 us (63%)
  matrix products  215 us (20%)
  blocking collectives  89 us (8%)
  local copies, waits for them, and re-layouts  37.1 us (4%)
  waiting for transfers between devices  19.4 us (2%)
  between operations  15 us (1%)
    another operation x7, other arithmetic, block_terms(): jax.scipy.linalg.solve_triangular(system, right_side, lower=True, unit_di...  636 us
    psum x1, blocking collectives, per_device(): latent_sum, context_sum = lax.psum((latent_part, context_part), 'sp')  63 us
    dot_general x23, matrix products, compose(): jnp.einsum('nmy,nyx->nmx', subsequent_map[0], preceding_map[1], precision...  41.6 us
    dot_general x16, matrix products, advance(): jnp.einsum('fga,fgo->fao', decayed_keys, fresh_values, precision=TOP_PREC...  29.1 us
    dot_general x16, matrix products, advance(): jnp.einsum('xui,xij->xuj', correction_term, carried_state, precision=TOP_...  25.6 us
    dot_general x23, matrix products, compose(): jnp.einsum('hkj,hjl->hkl', subsequent_map[0], preceding_map[0], precision...  25.5 us
  transfers between devices with their start and end apart: 7, of which 1 were waited for; matrix products, arithmetic and copies ran while one was open for 79% of the time, Pallas kernels for 0%

commit v1 on v0

v1 whole, which is shorter than its diff:
```python
import functools

import jax
import jax.numpy as jnp
from jax import lax
from jax.experimental import pallas as pl
from jax.experimental.pallas import tpu as pltpu
from jax.sharding import PartitionSpec as P

DK = 128
HALF = 128
EPSILON = 1e-06
TOP_PRECISION = lax.Precision.HIGHEST
BF = jnp.bfloat16
F32 = jnp.float32


def dot(a, b):
    return jnp.dot(a, b, preferred_element_type=F32)


def layer_norm(matrix):
    widened = matrix.astype(F32)
    centred = widened - jnp.mean(widened, axis=-1, keepdims=True)
    spread = jnp.mean(centred * centred, axis=-1, keepdims=True)
    return centred * lax.rsqrt(spread + EPSILON)


def modulate(matrix, shift_vec, scale_vec):
    return (layer_norm(matrix) * (1.0 + scale_vec) + shift_vec).astype(BF)


def invert_all(lowers):
    size = lowers[0].shape[0]
    rows = lax.broadcasted_iota(jnp.int32, (size, size), 0)
    cols = lax.broadcasted_iota(jnp.int32, (size, size), 1)
    apart = rows ^ cols
    eye = jnp.where(apart == 0, 1.0, 0.0)
    found = [eye - jnp.where(apart == 1, low, 0.0) for low in lowers]
    level = 1
    while (1 << level) < size:
        pick = (apart >> level) == 1
        narrow = [x.astype(BF) for x in found]
        first = [
            dot(x, jnp.where(pick, low, 0.0).astype(BF)).astype(BF)
            for x, low in zip(narrow, lowers)
        ]
        found = [f - dot(t, x) for f, t, x in zip(found, first, narrow)]
        level += 1
    return [x.astype(BF) for x in found]


def unit_rows(raw):
    wide = raw.astype(F32)
    return wide * lax.rsqrt(jnp.sum(wide * wide, axis=-1, keepdims=True) + EPSILON)


def order_masks(length, backward):
    rows = lax.broadcasted_iota(jnp.int32, (length, length), 0)
    cols = lax.broadcasted_iota(jnp.int32, (length, length), 1)
    return (rows < cols, rows <= cols) if backward else (rows > cols, rows >= cols)


def solve_pair(inverses, low, right, backward):
    h = HALF
    if backward:
        last = dot(inverses[1], right[h:].astype(BF)).astype(BF)
        rest = right[:h] - dot(low[:h, h:].astype(BF), last)
        return jnp.concatenate([dot(inverses[0], rest.astype(BF)).astype(BF), last], axis=0)
    head = dot(inverses[0], right[:h].astype(BF)).astype(BF)
    rest = right[h:] - dot(low[h:, :h].astype(BF), head)
    return jnp.concatenate([head, dot(inverses[1], rest.astype(BF)).astype(BF)], axis=0)


def local_kernel(q_ref, k_ref, v_ref, col_ref, row_ref, map_ref, z_ref, y_ref):
    length = q_ref.shape[0]
    h = HALF
    query = q_ref[...]
    keys = unit_rows(k_ref[...])
    values = v_ref[...].astype(F32)
    keys_t = keys.T
    narrow_t = keys_t.astype(BF)
    gram = dot(keys.astype(BF), narrow_t)
    scores = dot(query, narrow_t)
    wide_query = query.astype(F32)
    lows, blocks, reads = [], [], []
    for e in range(2):
        along = col_ref[0, :, e : e + 1]
        across = row_ref[0, e : e + 1, :]
        strength = col_ref[0, :, 2 + e : 3 + e]
        strictly, inclusive = order_masks(length, e == 1)
        decay = jnp.exp(jnp.minimum(along - across, 0.0))
        low = jnp.where(strictly, gram * decay * strength, 0.0)
        lows.append(low)
        reads.append(jnp.where(inclusive, scores * decay, 0.0).astype(BF))
        blocks += [low[:h, :h], low[h:, h:]]
    inverses = invert_all(blocks)
    total = jnp.zeros((length, DK), F32)
    rows = lax.broadcasted_iota(jnp.int32, (DK, DK), 0)
    cols = lax.broadcasted_iota(jnp.int32, (DK, DK), 1)
    for e in range(2):
        along = col_ref[0, :, e : e + 1]
        across = row_ref[0, e : e + 1, :]
        strength = col_ref[0, :, 2 + e : 3 + e]
        grown = jnp.exp(along)
        right = jnp.concatenate([values * strength, keys * (strength * grown)], axis=1)
        solved = solve_pair(inverses[2 * e : 2 * e + 2], lows[e], right, e == 1)
        final = across[:, length - 1 :] if e == 0 else across[:, :1]
        decayed_t = (keys_t * jnp.exp(final - across)).astype(BF)
        both = dot(decayed_t, solved)
        linear = jnp.where(rows == cols, jnp.exp(final), 0.0) - both[:, DK:]
        map_ref[e, 0, 0] = linear.astype(BF)
        map_ref[e, 0, 1] = both[:, :DK].astype(BF)
        seen = dot(reads[e], solved)
        total = total + seen[:, :DK]
        z_ref[0, :, e * DK : (e + 1) * DK] = (wide_query * grown - seen[:, DK:]).astype(BF)
    y_ref[0] = total


def local_terms(q, k, v, col, row, heads, length):
    spec = pl.BlockSpec((length, DK), lambda i: (0, i))
    return pl.pallas_call(
        local_kernel,
        grid=(heads,),
        in_specs=[
            spec,
            spec,
            spec,
            pl.BlockSpec((1, length, 4), lambda i: (i, 0, 0)),
            pl.BlockSpec((1, 2, length), lambda i: (i, 0, 0)),
        ],
        out_specs=[
            pl.BlockSpec((2, 1, 2, DK, DK), lambda i: (0, i, 0, 0, 0)),
            pl.BlockSpec((1, length, 2 * DK), lambda i: (i, 0, 0)),
            pl.BlockSpec((1, length, DK), lambda i: (i, 0, 0)),
        ],
        out_shape=[
            jax.ShapeDtypeStruct((2, heads, 2, DK, DK), BF),
            jax.ShapeDtypeStruct((heads, length, 2 * DK), BF),
            jax.ShapeDtypeStruct((heads, length, DK), F32),
        ],
        cost_estimate=pl.CostEstimate(
            flops=heads * 400 * DK**3, bytes_accessed=heads * 2**20, transcendentals=0
        ),
        name="local_terms",
    )(q, k, v, col, row)


def state_of(raw_keys, raw_values, along, across, strength):
    length = raw_keys.shape[0]
    h = HALF
    keys = unit_rows(raw_keys)
    keys_t = keys.T
    gram = dot(keys.astype(BF), keys_t.astype(BF))
    strictly, _ = order_masks(length, False)
    decay = jnp.exp(jnp.minimum(along - across, 0.0))
    low = jnp.where(strictly, gram * decay * strength, 0.0)
    inverses = invert_all([low[:h, :h], low[h:, h:]])
    solved = solve_pair(inverses, low, raw_values.astype(F32) * strength, False)
    decayed_t = (keys_t * jnp.exp(across[:, length - 1 :] - across)).astype(BF)
    return dot(decayed_t, solved)


def context_kernel(k_ref, v_ref, col_ref, row_ref, out_ref):
    out_ref[0] = state_of(
        k_ref[0], v_ref[0], col_ref[0, :, 0:1], row_ref[0], col_ref[0, :, 1:2]
    )


def context_states(k, v, col, row):
    count, length = k.shape[:2]
    wide = pl.BlockSpec((1, length, DK), lambda i: (i, 0, 0))
    return pl.pallas_call(
        context_kernel,
        grid=(count,),
        in_specs=[
            wide,
            wide,
            pl.BlockSpec((1, length, 2), lambda i: (i, 0, 0)),
            pl.BlockSpec((1, 1, length), lambda i: (i, 0, 0)),
        ],
        out_specs=pl.BlockSpec((1, DK, DK), lambda i: (i, 0, 0)),
        out_shape=jax.ShapeDtypeStruct((count, DK, DK), F32),
        cost_estimate=pl.CostEstimate(
            flops=count * 100 * DK**3, bytes_accessed=count * 2**18, transcendentals=0
        ),
        name="context_states",
    )(k, v, col, row)


def scan_kernel(flag_ref, map_ref, start_ref, out_ref):
    count = map_ref.shape[0]
    back = flag_ref[0]
    state = start_ref[0]
    for lap in range(count):
        source = jnp.where(back == 1, count - 1 - lap, lap)
        narrow = state.astype(BF)
        out_ref[source] = narrow
        if lap < count - 1:
            state = dot(map_ref[source, 0], narrow) + map_ref[source, 1].astype(F32)


def scan_states(flag, maps, start):
    return pl.pallas_call(
        scan_kernel,
        in_specs=[
            pl.BlockSpec(memory_space=pltpu.SMEM),
            pl.BlockSpec(memory_space=pltpu.VMEM),
            pl.BlockSpec(memory_space=pltpu.VMEM),
        ],
        out_specs=pl.BlockSpec(memory_space=pltpu.VMEM),
        out_shape=jax.ShapeDtypeStruct((maps.shape[0], DK, DK), BF),
        name="scan_states",
    )(flag, maps, start)


def read_kernel(z_ref, y_ref, s_ref, gain_ref, out_ref):
    state = s_ref[...].reshape(2 * DK, DK)
    summed = dot(z_ref[0], state) + y_ref[0]
    spread = jnp.mean(summed * summed, axis=-1, keepdims=True)
    out_ref[...] = (summed * lax.rsqrt(spread + EPSILON) * gain_ref[...]).astype(BF)


def read_out(z, y, states, gain):
    heads, length = z.shape[:2]
    return pl.pallas_call(
        read_kernel,
        grid=(heads,),
        in_specs=[
            pl.BlockSpec((1, length, 2 * DK), lambda i: (i, 0, 0)),
            pl.BlockSpec((1, length, DK), lambda i: (i, 0, 0)),
            pl.BlockSpec((2, 1, DK, DK), lambda i: (0, i, 0, 0)),
            pl.BlockSpec((1, DK), lambda i: (0, 0)),
        ],
        out_specs=pl.BlockSpec((length, DK), lambda i: (0, i)),
        out_shape=jax.ShapeDtypeStruct((length, heads * DK), BF),
        name="read_out",
    )(z, y, states, gain)


def gather_rows(matrix, axis):
    if lax.axis_size(axis) != 2:
        return lax.all_gather(matrix, axis, axis=0, tiled=True)
    other = lax.ppermute(matrix, axis, [(0, 1), (1, 0)])
    first = lax.axis_index(axis) == 0
    return jnp.concatenate(
        [jnp.where(first, matrix, other), jnp.where(first, other, matrix)], axis=0
    )


def scatter_sum(normed, weight, axis):
    if lax.axis_size(axis) != 2:
        return lax.psum_scatter(
            dot(normed, weight).astype(BF), axis, scatter_dimension=0, tiled=True
        ).astype(F32)
    rows = normed.shape[0] // 2
    mine = lax.axis_index(axis)
    theirs = dot(lax.dynamic_slice_in_dim(normed, (1 - mine) * rows, rows, 0), weight)
    arrived = lax.ppermute(theirs.astype(BF), axis, [(0, 1), (1, 0)])
    own = dot(lax.dynamic_slice_in_dim(normed, mine * rows, rows, 0), weight)
    return own + arrived.astype(F32)


def running_sums(decay):
    length = decay.shape[0]
    rows = lax.broadcasted_iota(jnp.int32, (length, length), 0)
    cols = lax.broadcasted_iota(jnp.int32, (length, length), 1)
    ahead = jnp.where(rows >= cols, 1.0, 0.0)
    return jnp.dot(ahead, decay, precision=TOP_PRECISION)


def per_device(
    latent,
    condition,
    context,
    context_condition_vector,
    modulation_matrix,
    query_matrix,
    key_matrix,
    value_matrix,
    decay_input_weight,
    write_strength_weight,
    head_decay_rate,
    write_strength_bias,
    context_write_offset_bias,
    log_spike_added,
    head_norm_gain,
    output_matrix,
):
    sp_index = lax.axis_index("sp")
    tp_index = lax.axis_index("tp")
    sp_count = lax.axis_size("sp")
    rows_part = modulation_matrix.shape[1]
    mod_float = modulation_matrix.astype(F32)
    signals = jnp.stack([jax.nn.silu(condition), jax.nn.silu(context_condition_vector)])
    signals = lax.dynamic_slice_in_dim(signals, sp_index * rows_part, rows_part, 1)
    latent_part = jnp.sum(mod_float * signals[0][None, :, None], axis=1)
    context_part = jnp.sum(mod_float[:2] * signals[1][None, :, None], axis=1)
    factors = lax.psum(jnp.concatenate([latent_part, context_part], axis=0), "sp")
    factors = lax.all_gather(factors, "tp", axis=1, tiled=True)

    hidden = gather_rows(modulate(latent, factors[0], factors[1]), "tp")
    context_own = modulate(context, factors[3], factors[4])
    length = hidden.shape[0]
    context_rows = context_own.shape[0]
    heads = query_matrix.shape[1] // DK
    pairs = 2 * heads
    leading = tp_index * pairs

    def columns(matrix):
        return lax.dynamic_slice_in_dim(matrix, leading, pairs, matrix.ndim - 1)

    gate_weight = jnp.concatenate(
        [columns(decay_input_weight), columns(write_strength_weight)], axis=1
    )
    rows_all = jnp.concatenate([hidden, context_own], axis=0)
    queries = dot(hidden, query_matrix).astype(BF)
    keys_raw = dot(rows_all, key_matrix).astype(BF)
    values = dot(rows_all, value_matrix).astype(BF)
    gates = dot(rows_all, gate_weight).astype(BF)

    decay_rates = columns(head_decay_rate)
    write_biases = columns(write_strength_bias)
    context_biases = write_biases + columns(context_write_offset_bias)

    latent_gates = gates[:length].astype(F32)
    log_decay = -decay_rates * jax.nn.softplus(latent_gates[:, :pairs]) + columns(log_spike_added)
    strength = jax.nn.sigmoid(latent_gates[:, pairs:] + write_biases)
    ahead = running_sums(log_decay)
    back = jnp.sum(log_decay, axis=0, keepdims=True) - ahead + log_decay
    forward_column = (jnp.arange(pairs) % 2 == 0)[None, :]
    summed_log = jnp.where(forward_column, ahead, back)
    by_head = summed_log.reshape(length, heads, 2)
    col = jnp.concatenate([by_head, strength.reshape(length, heads, 2)], axis=2).transpose(1, 0, 2)
    row = by_head.transpose(1, 2, 0)
    maps, z, y = local_terms(queries, keys_raw, values, col, row, heads, length)

    context_keys = keys_raw[length:].reshape(context_rows, heads, DK)
    context_values = values[length:].reshape(context_rows, heads, DK)
    context_gates = gates[length:].reshape(context_rows, 2, heads, 2)
    wide = jnp.concatenate([context_keys, context_values], axis=2).transpose(1, 0, 2)
    narrow = context_gates.transpose(3, 2, 0, 1)
    packed = jnp.concatenate(
        [jnp.broadcast_to(wide[None], (2,) + wide.shape), narrow], axis=3
    ).reshape(pairs, context_rows, 2 * DK + 2)
    by_pair = lambda vec: vec.reshape(heads, 2).T.reshape(pairs)
    rates_p, biases_p = by_pair(decay_rates), by_pair(context_biases)

    def context_start(rows, rates, biases, backward):
        rows = jnp.where(backward[:, None, None], rows[:, ::-1], rows)
        raw = rows[:, :, 2 * DK :].astype(F32)
        logs = -rates[:, None] * jax.nn.softplus(raw[:, :, 0])
        power = jax.nn.sigmoid(raw[:, :, 1] + biases[:, None])
        sums = running_sums(logs.T)
        cols = jnp.stack([sums.T, power], axis=2)
        return context_states(
            rows[:, :, :DK], rows[:, :, DK : 2 * DK], cols, sums.T[:, None, :]
        )

    if pairs == sp_count:
        rows = lax.all_to_all(packed, "sp", 0, 0, tiled=True).reshape(1, -1, 2 * DK + 2)
        is_back = (sp_index >= heads).reshape(1)
        take = lambda vec: lax.dynamic_slice_in_dim(vec, sp_index, 1, 0)
        start = context_start(rows, take(rates_p), take(biases_p), is_back)
        arrived = lax.all_to_all(maps.reshape(pairs, 2, DK, DK), "sp", 0, 0, tiled=True)
        prefixes = scan_states(is_back.astype(jnp.int32), arrived, start)
        states = lax.all_to_all(prefixes, "sp", 0, 0, tiled=True).reshape(2, heads, DK, DK)
    else:
        rows = lax.all_gather(packed, "sp", axis=1, tiled=True)
        start = context_start(rows, rates_p, biases_p, jnp.arange(pairs) >= heads)
        start = start.reshape(2, heads, DK, DK)
        gathered = lax.all_gather(maps, "sp")

        def run(e):
            laps = sp_count - 1 - sp_index if e else sp_index

            def one(lap, state):
                source = sp_count - 1 - lap if e else lap
                linear, offset = [
                    lax.dynamic_index_in_dim(gathered[:, e, :, i], source, 0, False)
                    for i in range(2)
                ]
                moved = jnp.einsum(
                    "hij,hjk->hik", linear, state.astype(BF), preferred_element_type=F32
                )
                return moved + offset.astype(F32)

            return lax.fori_loop(0, laps, one, start[e])

        states = jnp.stack([run(0), run(1)]).astype(BF)

    normed = read_out(z, y, states, head_norm_gain[None, :])
    branch = scatter_sum(normed, output_matrix, "tp")
    return (latent.astype(F32) + factors[2] * branch).astype(BF)


def solution(mesh):
    in_specs = (
        P(("sp", "tp"), None),
        P(),
        P("sp", None),
        P(),
        P(None, "sp", "tp"),
        P(None, "tp"),
        P(None, "tp"),
        P(None, "tp"),
        P(),
        P(),
        P(),
        P(),
        P(),
        P("sp", None),
        P(),
        P("tp", None),
    )
    out_specs = P(("sp", "tp"), None)
    return jax.shard_map(
        per_device, mesh=mesh, in_specs=in_specs, out_specs=out_specs, check_vma=False
    )
```

time: 1060 us -> 203 us (0.19); the launches traced: 1050 us -> 203 us
  other arithmetic: 667 us -> 6.48 us
  matrix products: 215 us -> 12.8 us
  Pallas kernels: 0 us -> 40.3 us
  local copies, waits for them, and re-layouts: 37.1 us -> 7.29 us
  waiting for transfers between devices: 19.4 us -> 47.4 us
  blocking collectives: 89 us -> 67.9 us
  starting transfers between devices: 0.25 us -> 19.4 us
  between operations: 15 us -> 1.08 us
    another operation x11 -> x2, other arithmetic: 640 us -> 0.85 us  [the longest x1 0.77 us: context_start(): cols = jnp.stack([sums.T, power], axis=2)]
    dot_general x118 -> x8, matrix products: 207 us -> 12.8 us  [the longest x6 12.1 us: dot(): return jnp.dot(a, b, preferred_element_type=F32)]
    pallas_call x0 -> x4, Pallas kernels: none -> 40.3 us  [the longest x1 26 us: local_terms(): pl.pallas_call(local_kernel, grid=(heads,), in_specs=[spec, spec, spec, p...]
    all_to_all x0 -> x3, waiting for transfers between devices: none -> 27.8 us  [the longest x1 14.3 us: per_device(): lax.all_to_all(prefixes, 'sp', 0, 0, tiled=True).reshape(2, heads, DK, DK)]
    all_gather x3 -> x1, blocking collectives: 26 us -> 4.92 us  [per_device(): factors = lax.all_gather(factors, 'tp', axis=1, tiled=True)]
    ppermute x0 -> x2, waiting for transfers between devices: none -> 19.5 us  [the longest x1 12.5 us: scatter_sum(): arrived = lax.ppermute(theirs.astype(BF), axis, [(0, 1), (1, 0)])]
    reduce_scatter x1 -> x0, waiting for transfers between devices: 19.2 us -> none  [per_device(): lax.psum_scatter(jnp.dot(normed, output_matrix, preferred_element_type=jn...]
    all_to_all x0 -> x3, starting transfers between devices: none -> 16.3 us  [the longest x1 6.79 us: per_device(): lax.all_to_all(prefixes, 'sp', 0, 0, tiled=True).reshape(2, heads, DK, DK)]
  transfers between devices with their start and end apart: 7 -> 5, of which waited for: 1 -> 4; matrix products, arithmetic and copies ran while one was open for 79% -> 3% of each run, Pallas kernels for 0% -> 15%
where the time goes in v1:
time: 203 us
  blocking collectives  67.9 us (33%)
  waiting for transfers between devices  47.4 us (23%)
  Pallas kernels  40.3 us (20%)
  starting transfers between devices  19.4 us (10%)
  matrix products  12.8 us (6%)
  local copies, waits for them, and re-layouts  7.29 us (4%)
  other arithmetic  6.48 us (3%)
    psum x1, blocking collectives, per_device(): lax.psum(jnp.concatenate([latent_part, context_part], axis=0), 'sp')  63 us
    pallas_call x1, Pallas kernels, local_terms(): pl.pallas_call(local_kernel, grid=(heads,), in_specs=[spec, spec, spec, p...  26 us
    all_to_all x1, waiting for transfers between devices, per_device(): lax.all_to_all(prefixes, 'sp', 0, 0, tiled=True).reshape(2, heads, DK, DK)  14.3 us
    all_to_all x1, waiting for transfers between devices, per_device(): lax.all_to_all(maps.reshape(pairs, 2, DK, DK), 'sp', 0, 0, tiled=True)  13.6 us
    ppermute x1, waiting for transfers between devices, scatter_sum(): arrived = lax.ppermute(theirs.astype(BF), axis, [(0, 1), (1, 0)])  12.5 us
    dot_general x6, matrix products, dot(): return jnp.dot(a, b, preferred_element_type=F32)  12.1 us
    ppermute x1, waiting for transfers between devices, gather_rows(): other = lax.ppermute(matrix, axis, [(0, 1), (1, 0)])  7.06 us
    all_to_all x1, starting transfers between devices, per_device(): lax.all_to_all(prefixes, 'sp', 0, 0, tiled=True).reshape(2, heads, DK, DK)  6.79 us
  transfers between devices with their start and end apart: 5, of which 4 were waited for; matrix products, arithmetic and copies ran while one was open for 3% of the time, Pallas kernels for 15%

profile of v1, /device:TPU:0, one launch (start us, length us, event | category | flops | bytes accessed | tf_op | source)
XLA Modules:
  0.0 202.6 jit_solution(11491202536705972430)
XLA Ops:
  0.0 1.4 convert_element_type.49
  2.0 63.0 %psum.7 = f32[5,1024]{1,0:T(8,128)S(1)} all-reduce(f32[5,1024]{1,0:T(8,128)S(1)} %pad_maximum_fusion.3), channel_id=1, replica_groups=mesh['sp'=16,'tp'=2] {'sp'}, use_global_device_ids=true, to_apply=%region_2.3 | all-reduce | flops 5120 | bytes 40960 | tf_op jit(solution)/shard_map/psum | solution.py:299
  65.0 4.9 %all_gather.3 = f32[5,2048]{1,0:T(8,128)S(1)} all-gather(f32[5,1024]{1,0:T(8,128)S(1)} %psum.7), channel_id=1, replica_groups=mesh['sp'=16,'tp'=2] {'tp'}, dimensions={1}, use_global_device_ids=true | all-gather | bytes 61440 | tf_op jit(solution)/shard_map/all_gather | solution.py:300
  70.9 1.6 collective-permute-start
  73.1 7.1 %collective-permute-done = bf16[128,2048]{1,0:T(8,128)(2,1)S(1)} collective-permute-done((bf16[128,2048]{1,0:T(8,128)(2,1)S(1)}, bf16[128,2048]{1,0:T(8,128)(2,1)S(1)}, u32[]{:S(2)}, u32[]{:S(2)}) %collective-permute-start) | collective-permute-done | bytes 524320 | tf_op jit(solution)/shard_map/ppermute | solution.py:244
  80.1 0.5 broadcast_select_fusion.1
  81.2 2.1 %convolution_convert_fusion.3.q_ref = bf16[256,1024]{1,0:T(8,128)(2,1)} fusion(bf16[2048,1024]{1,0:T(8,128)(2,1)S(1)} %copy-done.19, bf16[128,2048]{1,0:T(8,128)(2,1)S(1)} %get-tuple-element.16, bf16[128,2048]{1,0:T(8,128)(2,1)S(1)} %get-tuple-element.15), kind=kOutput, calls=%fused_computation.7 | convolution fusion | flops 1076101120 | bytes 5767168 | tf_op jit(solution)/shard_map/dot_general | solution.py:19
  83.4 1.3 convolution_convert_fusion.2.k_ref
  84.7 0.8 copy-done.21
  85.6 1.3 convolution_convert_fusion.1.v_ref
  87.6 1.4 copy.41.col_ref
  89.2 0.7 pad_maximum_fusion.1
  90.0 3.5 %all-to-all-start.1 = ((bf16[16,16,258]{2,1,0:T(8,128)(2,1)}), bf16[16,16,258]{2,1,0:T(8,128)(2,1)S(1)}, u32[]{:S(2)}, u32[]{:S(2)}) async-start(bf16[16,16,258]{2,1,0:T(8,128)(2,1)} %bitcast.16), calls=%async_computation.1 | async-start | bytes 393216 | tf_op jit(solution)/shard_map/all_to_all | solution.py:361
  93.5 26.0 %local_terms.1 = (bf16[2,8,2,128,128]{4,3,2,1,0:T(8,128)(2,1)}, bf16[8,256,256]{2,1,0:T(8,128)(2,1)}, f32[8,256,128]{2,1,0:T(8,128)}) custom-call(bf16[256,1024]{1,0:T(8,128)(2,1)} %convolution_convert_fusion.3.q_ref, bf16[272,1024]{1,0:T(8,128)(2,1)} %copy-done.13, bf16[272,1024]{1,0:T(8,128)(2,1)} %copy-done.14, f32[8,256,4]{2,1,0:T(8,128)} %copy.41.col_ref, ...), custom_call_target="tpu_custom_call" | custom-call | flops 6710886400 | bytes 8388608 | tf_op jit(solution)/shard_map/local_terms/pallas_call | solution.py:122
  119.5 6.0 %all-to-all-start = ((bf16[16,2,128,128]{3,2,1,0:T(8,128)(2,1)}), bf16[16,2,128,128]{3,2,1,0:T(8,128)(2,1)S(1)}, u32[]{:S(2)}, u32[]{:S(2)}) async-start(bf16[16,2,128,128]{3,2,1,0:T(8,128)(2,1)} %bitcast.56), calls=%async_computation | async-start | bytes 2097152 | tf_op jit(solution)/shard_map/all_to_all | solution.py:365
  126.0 0.6 dynamic_slice.41
  126.6 0.6 dynamic_slice.39
  128.1 0.8 slice_reduce_fusion
  129.5 0.8 pad_maximum_fusion.2.col_ref
  130.2 0.7 fusion.59
  130.9 3.9 %context_states.1.start_ref = f32[1,128,128]{2,1,0:T(8,128)} custom-call(bf16[1,256,128]{2,1,0:T(8,128)(2,1)} %get-tuple-element.18.k_ref, bf16[1,256,128]{2,1,0:T(8,128)(2,1)} %get-tuple-element.17.v_ref, f32[1,256,2]{2,1,0:T(8,128)} %pad_maximum_fusion.2.col_ref, f32[1,1,256]{2,1,0:T(1,128)} %bitcast.73), custom_call_target="tpu_custom_call" | custom-call | flops 209715200 | bytes 262144 | tf_op jit(solution)/shard_map/context_states/pallas_call | solution.py:173
  134.8 13.6 %all-to-all-done.map_ref = bf16[16,2,128,128]{3,2,1,0:T(8,128)(2,1)S(1)} async-done(((bf16[16,2,128,128]{3,2,1,0:T(8,128)(2,1)}), bf16[16,2,128,128]{3,2,1,0:T(8,128)(2,1)S(1)}, u32[]{:S(2)}, u32[]{:S(2)}) %all-to-all-start) | async-done | bytes 1048608 | tf_op jit(solution)/shard_map/all_to_all | solution.py:365
  148.4 1.0 copy-done.1
  149.3 4.0 %scan_states.1 = bf16[16,128,128]{2,1,0:T(8,128)(2,1)} custom-call(s32[1]{0:T(128)} %bitcast.11.flag_ref, bf16[16,2,128,128]{3,2,1,0:T(8,128)(2,1)} %copy-done.1, f32[1,128,128]{2,1,0:T(8,128)} %context_states.1.start_ref), custom_call_target="tpu_custom_call" | custom-call | tf_op jit(solution)/shard_map/scan_states/pallas_call | solution.py:204
  153.4 6.8 %all-to-all-start.2 = ((bf16[16,128,128]{2,1,0:T(8,128)(2,1)}), bf16[16,128,128]{2,1,0:T(8,128)(2,1)S(1)}, u32[]{:S(2)}, u32[]{:S(2)}) async-start(bf16[16,128,128]{2,1,0:T(8,128)(2,1)} %scan_states.1), calls=%async_computation.2 | async-start | bytes 1048576 | tf_op jit(solution)/shard_map/all_to_all | solution.py:367
  160.2 14.3 %all-to-all-done.2 = bf16[16,128,128]{2,1,0:T(8,128)(2,1)S(1)} async-done(((bf16[16,128,128]{2,1,0:T(8,128)(2,1)}), bf16[16,128,128]{2,1,0:T(8,128)(2,1)S(1)}, u32[]{:S(2)}, u32[]{:S(2)}) %all-to-all-start.2) | async-done | bytes 524320 | tf_op jit(solution)/shard_map/all_to_all | solution.py:367
  174.4 0.8 copy-done.4
  175.2 6.4 %read_out.1 = bf16[256,1024]{1,0:T(8,128)(2,1)} custom-call(bf16[8,256,256]{2,1,0:T(8,128)(2,1)} %get-tuple-element.8.z_ref, f32[8,256,128]{2,1,0:T(8,128)} %get-tuple-element.9.y_ref, bf16[2,8,128,128]{3,2,1,0:T(8,128)(2,1)} %bitcast.53, f32[1,128]{1,0:T(1,128)} %bitcast.75), custom_call_target="tpu_custom_call" | custom-call | tf_op jit(solution)/shard_map/read_out/pallas_call | solution.py:226
  181.6 3.0 %convolution_convert_fusion = bf16[128,2048]{1,0:T(8,128)(2,1)S(1)} fusion(bf16[1024,2048]{1,0:T(8,128)(2,1)} %param.31, bf16[256,1024]{1,0:T(8,128)(2,1)} %read_out.1, s32[]{:T(128)S(6)} %select_n.83), kind=kOutput, calls=%fused_computation | convolution fusion | flops 537133056 | bytes 4980740 | tf_op jit(solution)/shard_map/dot_general | solution.py:19
  184.7 1.6 collective-permute-start.1
  186.2 12.5 %collective-permute-done.1 = bf16[128,2048]{1,0:T(8,128)(2,1)S(1)} collective-permute-done((bf16[128,2048]{1,0:T(8,128)(2,1)S(1)}, bf16[128,2048]{1,0:T(8,128)(2,1)S(1)}, u32[]{:S(2)}, u32[]{:S(2)}) %collective-permute-start.1) | collective-permute-done | bytes 524320 | tf_op jit(solution)/shard_map/ppermute | solution.py:259
  198.7 3.9 %fusion.6 = bf16[128,2048]{1,0:T(8,128)(2,1)} fusion(bf16[128,2048]{1,0:T(8,128)(2,1)S(1)} %copy-done, bf16[128,2048]{1,0:T(8,128)(2,1)S(1)} %collective-permute-done.1, f32[2048]{0:T(1024)S(1)} %bitcast.64, bf16[1024,2048]{1,0:T(8,128)(2,1)} %param.31, bf16[256,1024]{1,0:T(8,128)(2,1)S(1)} %copy-done.3, s32[]{:T(128)S(6)} %select_n.82), kind=kOutput, calls=%fused_computation.16 | convolution fusion | flops 538443776 | bytes 6037508 | tf_op jit(solution)/shard_map/dot_general | solution.py:19
  (92 shorter events, 4.8 us)
Async XLA Ops:
  0.0 1.6 copy-start.2
  0.0 1.4 copy-start.10
  0.0 1.5 copy-start.11
  0.0 70.0 %copy-start = (bf16[128,2048]{1,0:T(8,128)(2,1)S(1)}, bf16[128,2048]{1,0:T(8,128)(2,1)}, u32[]{:S(2)}) copy-start(bf16[128,2048]{1,0:T(8,128)(2,1)} %param.16) | copy-start | bytes 1572868
  1.4 71.0 %copy-start.5 = (bf16[16,2048]{1,0:T(8,128)(2,1)S(1)}, bf16[16,2048]{1,0:T(8,128)(2,1)}, u32[]{:S(2)}) copy-start(bf16[16,2048]{1,0:T(8,128)(2,1)} %param.18) | copy-start | bytes 196612
  1.6 71.2 %copy-start.8 = (bf16[2048,32]{0,1:T(8,128)(2,1)S(1)}, bf16[2048,32]{0,1:T(8,128)(2,1)}, u32[]{:S(2)}) copy-start(bf16[2048,32]{0,1:T(8,128)(2,1)} %param.25) | copy-start | bytes 393220
  1.6 71.2 %copy-start.9 = (bf16[2048,32]{0,1:T(8,128)(2,1)S(1)}, bf16[2048,32]{0,1:T(8,128)(2,1)}, u32[]{:S(2)}) copy-start(bf16[2048,32]{0,1:T(8,128)(2,1)} %param.24) | copy-start | bytes 393220
  1.6 71.3 %copy-start.16 = (f32[32]{0:T(128)S(1)}, f32[32]{0:T(128)}, u32[]{:S(2)}) copy-start(f32[32]{0:T(128)} %param.28) | copy-start | bytes 388
  1.6 71.3 %copy-start.17 = (f32[32]{0:T(128)S(1)}, f32[32]{0:T(128)}, u32[]{:S(2)}) copy-start(f32[32]{0:T(128)} %param.27) | copy-start | bytes 388
  1.6 71.3 %copy-start.18 = (f32[32]{0:T(128)S(1)}, f32[32]{0:T(128)}, u32[]{:S(2)}) copy-start(f32[32]{0:T(128)} %param.26) | copy-start | bytes 388
  70.9 9.2 %collective-permute-start = (bf16[128,2048]{1,0:T(8,128)(2,1)S(1)}, bf16[128,2048]{1,0:T(8,128)(2,1)S(1)}, u32[]{:S(2)}, u32[]{:S(2)}) collective-permute-start(bf16[128,2048]{1,0:T(8,128)(2,1)S(1)} %fusion.5), channel_id=1, source_target_pairs={{0,1},{1,0},{2,3},{3,2},{4,5},{5,4},{6,7},{7,6},{8,9},{9,8},{10,11... | collective-permute-start | bytes 1572872 | tf_op jit(solution)/shard_map/ppermute | solution.py:244
  73.1 8.1 %copy-start.19 = (bf16[2048,1024]{1,0:T(8,128)(2,1)S(1)}, bf16[2048,1024]{1,0:T(8,128)(2,1)}, u32[]{:S(2)}) copy-start(bf16[2048,1024]{1,0:T(8,128)(2,1)} %param.21) | copy-start | bytes 12582916
  81.2 2.1 %copy-start.7 = (bf16[272,32]{0,1:T(8,128)(2,1)}, bf16[272,32]{0,1:T(8,128)(2,1)S(1)}, u32[]{:S(2)}) copy-start(bf16[272,32]{0,1:T(8,128)(2,1)S(1)} %convolution_convert_fusion.4) | copy-start | bytes 52228
  81.2 2.2 %copy-start.20 = (bf16[2048,1024]{1,0:T(8,128)(2,1)S(1)}, bf16[2048,1024]{1,0:T(8,128)(2,1)}, u32[]{:S(2)}) copy-start(bf16[2048,1024]{1,0:T(8,128)(2,1)} %param.22) | copy-start | bytes 12582916
  83.4 2.2 %copy-start.21 = (bf16[2048,1024]{1,0:T(8,128)(2,1)S(1)}, bf16[2048,1024]{1,0:T(8,128)(2,1)}, u32[]{:S(2)}) copy-start(bf16[2048,1024]{1,0:T(8,128)(2,1)} %param.23) | copy-start | bytes 12582916
  85.6 3.6 %copy-start.13 = (bf16[272,1024]{1,0:T(8,128)(2,1)}, bf16[272,1024]{1,0:T(8,128)(2,1)S(1)}, u32[]{:S(2)}) copy-start(bf16[272,1024]{1,0:T(8,128)(2,1)S(1)} %convolution_convert_fusion.2.k_ref) | copy-start | bytes 1671172
  85.6 1.4 copy-start.12
  85.6 3.4 %slice-start = ((bf16[272,32]{0,1:T(8,128)(2,1)}), bf16[16,32]{0,1:T(8,128)(2,1)S(1)}, s32[]{:S(2)}) async-start(bf16[272,32]{0,1:T(8,128)(2,1)} %copy-done.7), calls=%async_computation.3 | async-start | bytes 16384 | tf_op jit(solution)/shard_map/slice | solution.py:340
  86.9 6.6 %copy-start.14 = (bf16[272,1024]{1,0:T(8,128)(2,1)}, bf16[272,1024]{1,0:T(8,128)(2,1)S(1)}, u32[]{:S(2)}) copy-start(bf16[272,1024]{1,0:T(8,128)(2,1)S(1)} %convolution_convert_fusion.1.v_ref) | copy-start | bytes 1671172
  87.5 6.0 %copy-start.6 = (f32[256,8,2]{0,2,1:T(2,128)}, f32[256,8,2]{0,2,1:T(2,128)S(1)}, u32[]{:S(2)}) copy-start(f32[256,8,2]{0,2,1:T(2,128)S(1)} %reshape.125) | copy-start | bytes 49156
  90.0 29.5 %all-to-all-start.1 = ((bf16[16,16,258]{2,1,0:T(8,128)(2,1)}), bf16[16,16,258]{2,1,0:T(8,128)(2,1)S(1)}, u32[]{:S(2)}, u32[]{:S(2)}) async-start(bf16[16,16,258]{2,1,0:T(8,128)(2,1)} %bitcast.16), calls=%async_computation.1 | async-start | bytes 393216 | tf_op jit(solution)/shard_map/all_to_all | solution.py:361
  119.5 28.9 %all-to-all-start = ((bf16[16,2,128,128]{3,2,1,0:T(8,128)(2,1)}), bf16[16,2,128,128]{3,2,1,0:T(8,128)(2,1)S(1)}, u32[]{:S(2)}, u32[]{:S(2)}) async-start(bf16[16,2,128,128]{3,2,1,0:T(8,128)(2,1)} %bitcast.56), calls=%async_computation | async-start | bytes 2097152 | tf_op jit(solution)/shard_map/all_to_all | solution.py:365
  129.2 1.6 copy-start.15
  148.4 1.0 copy-start.1
  153.4 21.1 %all-to-all-start.2 = ((bf16[16,128,128]{2,1,0:T(8,128)(2,1)}), bf16[16,128,128]{2,1,0:T(8,128)(2,1)S(1)}, u32[]{:S(2)}, u32[]{:S(2)}) async-start(bf16[16,128,128]{2,1,0:T(8,128)(2,1)} %scan_states.1), calls=%async_computation.2 | async-start | bytes 1048576 | tf_op jit(solution)/shard_map/all_to_all | solution.py:367
  174.4 0.8 copy-start.4
  181.6 17.1 %copy-start.3 = (bf16[256,1024]{1,0:T(8,128)(2,1)S(1)}, bf16[256,1024]{1,0:T(8,128)(2,1)}, u32[]{:S(2)}) copy-start(bf16[256,1024]{1,0:T(8,128)(2,1)} %read_out.1) | copy-start | bytes 1572868
  184.7 14.0 %collective-permute-start.1 = (bf16[128,2048]{1,0:T(8,128)(2,1)S(1)}, bf16[128,2048]{1,0:T(8,128)(2,1)S(1)}, u32[]{:S(2)}, u32[]{:S(2)}) collective-permute-start(bf16[128,2048]{1,0:T(8,128)(2,1)S(1)} %convolution_convert_fusion), channel_id=1, source_target_pairs={{0,1},{1,0},{2,3},{3,2},{4,5},{5,4},{6,7},{7,6},{8,9},{9,8},{10,11... | collective-permute-start | bytes 1572872 | tf_op jit(solution)/shard_map/ppermute | solution.py:259

commit v2 on v1

--- a/solution.py
+++ b/solution.py
@@ -188,30 +188,225 @@
     )(k, v, col, row)
 
 
-def scan_kernel(flag_ref, map_ref, start_ref, out_ref):
-    count = map_ref.shape[0]
-    back = flag_ref[0]
+MESH = pl.DeviceIdType.MESH
+
+
+def greet(peers):
+    barrier = pltpu.get_barrier_semaphore()
+    for peer in peers:
+        pl.semaphore_signal(barrier, inc=1, device_id=peer, device_id_type=MESH)
+    pl.semaphore_wait(barrier, len(peers))
+
+
+def factor_kernel(n, m, x_ref, out_ref, parts, block, sent_a, got_a, sent_b, got_b):
+    width = 128
+    reducers = x_ref.shape[1] // width
+    me, side = lax.axis_index("sp"), lax.axis_index("tp")
+    flat = me * m + side
+    others = []
+    for step in range(1, n * m):
+        p = lax.rem(flat + step, n * m)
+        others.append((p // m, lax.rem(p, m)))
+    greet(others)
+
+    def part(c):
+        return pltpu.make_async_remote_copy(
+            src_ref=x_ref.at[:, pl.ds(c * width, width)],
+            dst_ref=parts.at[me],
+            send_sem=sent_a.at[c],
+            recv_sem=got_a.at[me],
+            device_id=(c, side),
+            device_id_type=MESH,
+        )
+
+    for c in range(reducers):
+
+        @pl.when(me != c)
+        def _():
+            part(c).start()
+
+        @pl.when(me == c)
+        def _():
+            parts[c] = x_ref[:, c * width : (c + 1) * width]
+
+    slot = side * reducers + me
+
+    def whole(step, where):
+        return pltpu.make_async_remote_copy(
+            src_ref=block,
+            dst_ref=out_ref.at[:, pl.ds(pl.multiple_of(where * width, width), width)],
+            send_sem=sent_b.at[step],
+            recv_sem=got_b.at[where],
+            device_id=others[step],
+            device_id_type=MESH,
+        )
+
+    @pl.when(me < reducers)
+    def _():
+        for s in range(n):
+
+            @pl.when(me != s)
+            def _():
+                pltpu.make_async_remote_copy(
+                    src_ref=block,
+                    dst_ref=parts.at[s],
+                    send_sem=sent_a.at[0],
+                    recv_sem=got_a.at[s],
+                    device_id=others[0],
+                    device_id_type=MESH,
+                ).wait_recv()
+
+        total = parts[0]
+        for s in range(1, n):
+            total = total + parts[s]
+        block[...] = total
+        for step in range(n * m - 1):
+            whole(step, slot).start()
+        out_ref[:, pl.ds(pl.multiple_of(slot * width, width), width)] = total
+
+    for where in range(m * reducers):
+
+        @pl.when(jnp.logical_or(me != where % reducers, side != where // reducers))
+        def _():
+            whole(0, where).wait_recv()
+
+    for c in range(reducers):
+
+        @pl.when(me != c)
+        def _():
+            part(c).wait_send()
+
+    @pl.when(me < reducers)
+    def _():
+        for step in range(n * m - 1):
+            whole(step, slot).wait_send()
+
+
+def sum_factors(part):
+    n, m = lax.axis_size("sp"), lax.axis_size("tp")
+    rows, columns = part.shape
+    reducers = columns // 128
+    return pl.pallas_call(
+        functools.partial(factor_kernel, n, m),
+        in_specs=[pl.BlockSpec(memory_space=pltpu.VMEM)],
+        out_specs=pl.BlockSpec(memory_space=pltpu.VMEM),
+        out_shape=jax.ShapeDtypeStruct((rows, m * columns), F32),
+        scratch_shapes=[
+            pltpu.VMEM((n, rows, 128), F32),
+            pltpu.VMEM((rows, 128), F32),
+            pltpu.SemaphoreType.DMA((reducers,)),
+            pltpu.SemaphoreType.DMA((n,)),
+            pltpu.SemaphoreType.DMA((n * m - 1,)),
+            pltpu.SemaphoreType.DMA((m * reducers,)),
+        ],
+        compiler_params=pltpu.CompilerParams(collective_id=1, has_side_effects=True),
+        name="sum_factors",
+    )(part)
+
+
+def swap_kernel(n, x_ref, out_ref, sent, got):
+    me, side = lax.axis_index("sp"), lax.axis_index("tp")
+    peers = [lax.rem(me + step, n) for step in range(1, n)]
+    greet([(p, side) for p in peers])
+    copies = []
+    for step, p in enumerate(peers):
+        copy = pltpu.make_async_remote_copy(
+            src_ref=x_ref.at[p],
+            dst_ref=out_ref.at[me],
+            send_sem=sent.at[step],
+            recv_sem=got.at[step],
+            device_id=(p, side),
+            device_id_type=MESH,
+        )
+        copy.start()
+        copies.append(copy)
+    out_ref[me] = x_ref[me]
+    for copy in copies:
+        copy.wait()
+
+
+def swap_blocks(x):
+    n = lax.axis_size("sp")
+    return pl.pallas_call(
+        functools.partial(swap_kernel, n),
+        in_specs=[pl.BlockSpec(memory_space=pltpu.VMEM)],
+        out_specs=pl.BlockSpec(memory_space=pltpu.VMEM),
+        out_shape=jax.ShapeDtypeStruct(x.shape, x.dtype),
+        scratch_shapes=[pltpu.SemaphoreType.DMA((n - 1,)), pltpu.SemaphoreType.DMA((n - 1,))],
+        compiler_params=pltpu.CompilerParams(collective_id=2, has_side_effects=True),
+        name="swap_blocks",
+    )(x)
+
+
+def exchange_kernel(
+    n, map_ref, start_ref, out_ref, held, ready, sent_a, got_a, sent_b, got_b
+):
+    me, side = lax.axis_index("sp"), lax.axis_index("tp")
+    peers = [lax.rem(me + step, n) for step in range(1, n)]
+    greet([(p, side) for p in peers])
+
+    def outward(p, source):
+        return pltpu.make_async_remote_copy(
+            src_ref=map_ref.at[p],
+            dst_ref=held.at[source],
+            send_sem=sent_a.at[p],
+            recv_sem=got_a.at[source],
+            device_id=(p, side),
+            device_id_type=MESH,
+        )
+
+    def homeward(p, source):
+        return pltpu.make_async_remote_copy(
+            src_ref=ready.at[p],
+            dst_ref=out_ref.at[source],
+            send_sem=sent_b.at[p],
+            recv_sem=got_b.at[source],
+            device_id=(p, side),
+            device_id_type=MESH,
+        )
+
+    for p in peers:
+        outward(p, me).start()
+    held[me] = map_ref[me]
+    back = me // (n // 2)
     state = start_ref[0]
-    for lap in range(count):
-        source = jnp.where(back == 1, count - 1 - lap, lap)
+    for lap in range(n):
+        source = lap + back * (n - 1 - 2 * lap)
         narrow = state.astype(BF)
-        out_ref[source] = narrow
-        if lap < count - 1:
-            state = dot(map_ref[source, 0], narrow) + map_ref[source, 1].astype(F32)
-
-
-def scan_states(flag, maps, start):
+        ready[source] = narrow
+
+        @pl.when(source != me)
+        def _():
+            homeward(source, me).start()
+            outward(source, source).wait_recv()
+
+        if lap < n - 1:
+            state = dot(held[source, 0], narrow) + held[source, 1].astype(F32)
+    out_ref[me] = ready[me]
+    for p in peers:
+        outward(p, me).wait_send()
+        homeward(p, me).wait_send()
+        homeward(p, p).wait_recv()
+
+
+def exchange_states(maps, start):
+    n = lax.axis_size("sp")
     return pl.pallas_call(
-        scan_kernel,
-        in_specs=[
-            pl.BlockSpec(memory_space=pltpu.SMEM),
-            pl.BlockSpec(memory_space=pltpu.VMEM),
-            pl.BlockSpec(memory_space=pltpu.VMEM),
+        functools.partial(exchange_kernel, n),
+        in_specs=[pl.BlockSpec(memory_space=pltpu.VMEM)] * 2,
+        out_specs=pl.BlockSpec(memory_space=pltpu.VMEM),
+        out_shape=jax.ShapeDtypeStruct((n, DK, DK), BF),
+        scratch_shapes=[
+            pltpu.VMEM(maps.shape, BF),
+            pltpu.VMEM((n, DK, DK), BF),
+            pltpu.SemaphoreType.DMA((n,)),
+            pltpu.SemaphoreType.DMA((n,)),
+            pltpu.SemaphoreType.DMA((n,)),
+            pltpu.SemaphoreType.DMA((n,)),
         ],
-        out_specs=pl.BlockSpec(memory_space=pltpu.VMEM),
-        out_shape=jax.ShapeDtypeStruct((maps.shape[0], DK, DK), BF),
-        name="scan_states",
-    )(flag, maps, start)
+        compiler_params=pltpu.CompilerParams(collective_id=3, has_side_effects=True),
+        name="exchange_states",
+    )(maps, start)
 
 
 def read_kernel(z_ref, y_ref, s_ref, gain_ref, out_ref):
@@ -296,8 +491,12 @@
     signals = lax.dynamic_slice_in_dim(signals, sp_index * rows_part, rows_part, 1)
     latent_part = jnp.sum(mod_float * signals[0][None, :, None], axis=1)
     context_part = jnp.sum(mod_float[:2] * signals[1][None, :, None], axis=1)
-    factors = lax.psum(jnp.concatenate([latent_part, context_part], axis=0), "sp")
-    factors = lax.all_gather(factors, "tp", axis=1, tiled=True)
+    parts = jnp.concatenate([latent_part, context_part], axis=0)
+    whole_pairs = 2 * query_matrix.shape[1] // DK == sp_count
+    if whole_pairs and parts.shape[1] // 128 <= sp_count:
+        factors = sum_factors(jnp.pad(parts, ((0, 8 - parts.shape[0]), (0, 0))))
+    else:
+        factors = lax.all_gather(lax.psum(parts, "sp"), "tp", axis=1, tiled=True)
 
     hidden = gather_rows(modulate(latent, factors[0], factors[1]), "tp")
     context_own = modulate(context, factors[3], factors[4])
@@ -357,14 +556,13 @@
             rows[:, :, :DK], rows[:, :, DK : 2 * DK], cols, sums.T[:, None, :]
         )
 
-    if pairs == sp_count:
-        rows = lax.all_to_all(packed, "sp", 0, 0, tiled=True).reshape(1, -1, 2 * DK + 2)
+    if whole_pairs:
+        rows = swap_blocks(packed).reshape(1, -1, 2 * DK + 2)
         is_back = (sp_index >= heads).reshape(1)
         take = lambda vec: lax.dynamic_slice_in_dim(vec, sp_index, 1, 0)
         start = context_start(rows, take(rates_p), take(biases_p), is_back)
-        arrived = lax.all_to_all(maps.reshape(pairs, 2, DK, DK), "sp", 0, 0, tiled=True)
-        prefixes = scan_states(is_back.astype(jnp.int32), arrived, start)
-        states = lax.all_to_all(prefixes, "sp", 0, 0, tiled=True).reshape(2, heads, DK, DK)
+        states = exchange_states(maps.reshape(pairs, 2, DK, DK), start)
+        states = states.reshape(2, heads, DK, DK)
     else:
         rows = lax.all_gather(packed, "sp", axis=1, tiled=True)
         start = context_start(rows, rates_p, biases_p, jnp.arange(pairs) >= heads)

time: 203 us -> 164 us (0.81)
  blocking collectives: 67.9 us -> 0 us
  Pallas kernels: 40.3 us -> 106 us
  waiting for transfers between devices: 47.4 us -> 21.5 us
  starting transfers between devices: 19.4 us -> 3.1 us
  other arithmetic: 6.48 us -> 8.95 us
  matrix products: 12.8 us -> 14.9 us
    pallas_call x1 -> x3, Pallas kernels: 4.03 us -> 69.4 us  [the longest x1 43.6 us: exchange_states(): pl.pallas_call(functools.partial(exchange_kernel, n), in_specs=[pl.BlockS...]
    psum x1 -> x0, blocking collectives: 63 us -> none  [per_device(): lax.psum(jnp.concatenate([latent_part, context_part], axis=0), 'sp')]
    all_to_all x3 -> x0, waiting for transfers between devices: 27.8 us -> none  [the longest x1 14.3 us: per_device(): lax.all_to_all(prefixes, 'sp', 0, 0, tiled=True).reshape(2, heads, DK, DK)]
    all_to_all x3 -> x0, starting transfers between devices: 16.3 us -> none  [the longest x1 6.79 us: per_device(): lax.all_to_all(prefixes, 'sp', 0, 0, tiled=True).reshape(2, heads, DK, DK)]
    all_gather x1 -> x0, blocking collectives: 4.92 us -> none  [per_device(): factors = lax.all_gather(factors, 'tp', axis=1, tiled=True)]
    ppermute x1, waiting for transfers between devices: 7.06 us -> 9.47 us  [gather_rows(): other = lax.ppermute(matrix, axis, [(0, 1), (1, 0)])]
    dot_general x6, matrix products: 12.1 us -> 14.3 us  [dot(): return jnp.dot(a, b, preferred_element_type=F32)]
    rev x1, local copies, waits for them, and re-layouts: 0.26 us -> 2.41 us  [context_start(): rows = jnp.where(backward[:, None, None], rows[:, ::-1], rows)]
  transfers between devices with their start and end apart: 5 -> 2, of which waited for: 4 -> 2; matrix products, arithmetic and copies ran while one was open for 3% -> 1% of each run, Pallas kernels for 15% -> 0%
where the time goes in v2:
time: 164 us; the launch traced here: 163 us
  Pallas kernels  106 us (65%)
  waiting for transfers between devices  21.5 us (13%)
  matrix products  14.9 us (9%)
  other arithmetic  8.95 us (5%)
  local copies, waits for them, and re-layouts  7.52 us (5%)
  starting transfers between devices  3.1 us (2%)
    pallas_call x1, Pallas kernels, exchange_states(): pl.pallas_call(functools.partial(exchange_kernel, n), in_specs=[pl.BlockS...  43.6 us
    pallas_call x1, Pallas kernels, local_terms(): pl.pallas_call(local_kernel, grid=(heads,), in_specs=[spec, spec, spec, p...  26 us
    pallas_call x1, Pallas kernels, sum_factors(): pl.pallas_call(functools.partial(factor_kernel, n, m), in_specs=[pl.Block...  15.4 us
    dot_general x6, matrix products, dot(): return jnp.dot(a, b, preferred_element_type=F32)  14.3 us
    ppermute x1, waiting for transfers between devices, scatter_sum(): arrived = lax.ppermute(theirs.astype(BF), axis, [(0, 1), (1, 0)])  12 us
    pallas_call x1, Pallas kernels, swap_blocks(): pl.pallas_call(functools.partial(swap_kernel, n), in_specs=[pl.BlockSpec(...  10.4 us
    ppermute x1, waiting for transfers between devices, gather_rows(): other = lax.ppermute(matrix, axis, [(0, 1), (1, 0)])  9.47 us
    pallas_call x1, Pallas kernels, read_out(): pl.pallas_call(read_kernel, grid=(heads,), in_specs=[pl.BlockSpec((1, len...  6.39 us
  transfers between devices with their start and end apart: 2, of which 2 were waited for; matrix products, arithmetic and copies ran while one was open for 1% of the time, Pallas kernels for 0%

profile of v2, /device:TPU:0, one launch (start us, length us, event | category | flops | bytes accessed | tf_op | source)
XLA Modules:
  0.0 162.7 jit_solution(14105318365768743666)
XLA Ops:
  0.0 1.4 convert_element_type.46
  2.0 0.6 select_maximum_fusion.x_ref
  2.7 15.4 %sum_factors.1 = f32[8,2048]{1,0:T(8,128)} custom-call(f32[8,1024]{1,0:T(8,128)} %select_maximum_fusion.x_ref), custom_call_target="tpu_custom_call" | custom-call | tf_op jit(solution)/shard_map/sum_factors/pallas_call | solution.py:289
  18.1 1.1 fusion.60
  19.6 0.4 fusion.5
  20.1 1.5 collective-permute-start
  22.6 0.6 dynamic_slice.41
  23.2 0.6 dynamic_slice.39
  24.6 9.5 %collective-permute-done = bf16[128,2048]{1,0:T(8,128)(2,1)S(1)} collective-permute-done((bf16[128,2048]{1,0:T(8,128)(2,1)S(1)}, bf16[128,2048]{1,0:T(8,128)(2,1)S(1)}, u32[]{:S(2)}, u32[]{:S(2)}) %collective-permute-start) | collective-permute-done | bytes 524320 | tf_op jit(solution)/shard_map/ppermute | solution.py:439
  34.0 0.5 broadcast_select_fusion.1
  34.6 0.5 convolution_convert_fusion.4
  35.1 1.4 convolution_convert_fusion.2.k_ref
  36.5 0.8 copy-done.17
  37.3 1.3 convolution_convert_fusion.1.v_ref
  39.0 0.7 pad_maximum_fusion.1
  39.7 10.4 %swap_blocks.1 = bf16[16,16,258]{2,1,0:T(8,128)(2,1)} custom-call(bf16[16,16,258]{2,1,0:T(8,128)(2,1)} %bitcast.55), custom_call_target="tpu_custom_call" | custom-call | tf_op jit(solution)/shard_map/swap_blocks/pallas_call | solution.py:330
  50.0 2.4 %rev.3 = bf16[1,256,258]{2,1,0:T(8,128)(2,1)S(1)} reverse(bf16[1,256,258]{2,1,0:T(8,128)(2,1)} %bitcast.52), dimensions={1} | reverse | bytes 264192 | tf_op jit(solution)/shard_map/rev | solution.py:549
  52.5 1.0 broadcast_select_fusion.2
  53.4 0.7 fusion.59
  54.1 4.2 %convolution_convert_fusion.3.q_ref = bf16[256,1024]{1,0:T(8,128)(2,1)} fusion(bf16[2048,1024]{1,0:T(8,128)(2,1)} %param.21, bf16[128,2048]{1,0:T(8,128)(2,1)S(1)} %get-tuple-element.16, bf16[128,2048]{1,0:T(8,128)(2,1)S(1)} %get-tuple-element.15), kind=kOutput, calls=%fused_computation.7 | convolution fusion | flops 1076101120 | bytes 5767168 | tf_op jit(solution)/shard_map/dot_general | solution.py:19
  58.6 0.3 add_select_fusion
  59.0 1.3 copy.41.col_ref
  60.3 0.7 slice_reduce_fusion
  61.6 0.8 pad_maximum_fusion.2.col_ref
  62.3 26.0 %local_terms.1 = (bf16[2,8,2,128,128]{4,3,2,1,0:T(8,128)(2,1)}, bf16[8,256,256]{2,1,0:T(8,128)(2,1)}, f32[8,256,128]{2,1,0:T(8,128)}) custom-call(bf16[256,1024]{1,0:T(8,128)(2,1)} %convolution_convert_fusion.3.q_ref, bf16[272,1024]{1,0:T(8,128)(2,1)} %copy-done.10, bf16[272,1024]{1,0:T(8,128)(2,1)} %copy-done.11, f32[8,256,4]{2,1,0:T(8,128)} %copy.41.col_ref, ...), custom_call_target="tpu_custom_call" | custom-call | flops 6710886400 | bytes 8388608 | tf_op jit(solution)/shard_map/local_terms/pallas_call | solution.py:122
  88.3 3.9 %context_states.1.start_ref = f32[1,128,128]{2,1,0:T(8,128)} custom-call(bf16[1,256,128]{2,1,0:T(8,128)(2,1)} %get-tuple-element.18.k_ref, bf16[1,256,128]{2,1,0:T(8,128)(2,1)} %get-tuple-element.17.v_ref, f32[1,256,2]{2,1,0:T(8,128)} %pad_maximum_fusion.2.col_ref, f32[1,1,256]{2,1,0:T(1,128)} %bitcast.73), custom_call_target="tpu_custom_call" | custom-call | flops 209715200 | bytes 262144 | tf_op jit(solution)/shard_map/context_states/pallas_call | solution.py:173
  92.2 43.6 %exchange_states.1 = bf16[16,128,128]{2,1,0:T(8,128)(2,1)} custom-call(bf16[16,2,128,128]{3,2,1,0:T(8,128)(2,1)} %bitcast.54, f32[1,128,128]{2,1,0:T(8,128)} %context_states.1.start_ref), custom_call_target="tpu_custom_call" | custom-call | tf_op jit(solution)/shard_map/exchange_states/pallas_call | solution.py:394
  135.8 6.4 %read_out.1 = bf16[256,1024]{1,0:T(8,128)(2,1)} custom-call(bf16[8,256,256]{2,1,0:T(8,128)(2,1)} %get-tuple-element.8.z_ref, f32[8,256,128]{2,1,0:T(8,128)} %get-tuple-element.9.y_ref, bf16[2,8,128,128]{3,2,1,0:T(8,128)(2,1)} %bitcast.51, f32[1,128]{1,0:T(1,128)} %bitcast.75), custom_call_target="tpu_custom_call" | custom-call | tf_op jit(solution)/shard_map/read_out/pallas_call | solution.py:421
  142.2 3.0 %convolution_convert_fusion = bf16[128,2048]{1,0:T(8,128)(2,1)S(1)} fusion(bf16[1024,2048]{1,0:T(8,128)(2,1)} %param.31, bf16[256,1024]{1,0:T(8,128)(2,1)} %read_out.1, s32[]{:T(128)S(6)} %select_n.83), kind=kOutput, calls=%fused_computation | convolution fusion | flops 537133056 | bytes 4980740 | tf_op jit(solution)/shard_map/dot_general | solution.py:19
  145.3 1.6 collective-permute-start.1
  146.8 12.0 %collective-permute-done.1 = bf16[128,2048]{1,0:T(8,128)(2,1)S(1)} collective-permute-done((bf16[128,2048]{1,0:T(8,128)(2,1)S(1)}, bf16[128,2048]{1,0:T(8,128)(2,1)S(1)}, u32[]{:S(2)}, u32[]{:S(2)}) %collective-permute-start.1) | collective-permute-done | bytes 524320 | tf_op jit(solution)/shard_map/ppermute | solution.py:454
  158.8 3.9 %fusion.6 = bf16[128,2048]{1,0:T(8,128)(2,1)} fusion(bf16[128,2048]{1,0:T(8,128)(2,1)S(1)} %copy-done, bf16[128,2048]{1,0:T(8,128)(2,1)S(1)} %collective-permute-done.1, f32[2048]{0:T(1024)S(1)} %bitcast.64, bf16[1024,2048]{1,0:T(8,128)(2,1)} %param.31, bf16[256,1024]{1,0:T(8,128)(2,1)S(1)} %copy-done.2, s32[]{:T(128)S(6)} %select_n.82), kind=kOutput, calls=%fused_computation.16 | convolution fusion | flops 538443776 | bytes 6037508 | tf_op jit(solution)/shard_map/dot_general | solution.py:19
  (77 shorter events, 3.1 us)
Async XLA Ops:
  0.0 1.6 %copy-start.1 = (bf16[3,128,1024]{2,1,0:T(8,128)(2,1)S(1)}, bf16[3,128,1024]{2,1,0:T(8,128)(2,1)}, u32[]{:S(2)}) copy-start(bf16[3,128,1024]{2,1,0:T(8,128)(2,1)} %param.20) | copy-start | bytes 2359300
  0.0 1.5 copy-start.7
  0.0 1.5 copy-start.8
  0.0 19.2 %copy-start = (bf16[128,2048]{1,0:T(8,128)(2,1)S(1)}, bf16[128,2048]{1,0:T(8,128)(2,1)}, u32[]{:S(2)}) copy-start(bf16[128,2048]{1,0:T(8,128)(2,1)} %param.16) | copy-start | bytes 1572868
  1.4 20.2 %copy-start.3 = (bf16[16,2048]{1,0:T(8,128)(2,1)S(1)}, bf16[16,2048]{1,0:T(8,128)(2,1)}, u32[]{:S(2)}) copy-start(bf16[16,2048]{1,0:T(8,128)(2,1)} %param.18) | copy-start | bytes 196612
  1.4 20.5 %copy-start.13 = (f32[32]{0:T(128)S(1)}, f32[32]{0:T(128)}, u32[]{:S(2)}) copy-start(f32[32]{0:T(128)} %param.28) | copy-start | bytes 388
  1.4 20.5 %copy-start.14 = (f32[32]{0:T(128)S(1)}, f32[32]{0:T(128)}, u32[]{:S(2)}) copy-start(f32[32]{0:T(128)} %param.27) | copy-start | bytes 388
  1.5 20.5 %copy-start.15 = (f32[32]{0:T(128)S(1)}, f32[32]{0:T(128)}, u32[]{:S(2)}) copy-start(f32[32]{0:T(128)} %param.26) | copy-start | bytes 388
  1.5 22.9 %copy-start.5 = (bf16[2048,32]{0,1:T(8,128)(2,1)S(1)}, bf16[2048,32]{0,1:T(8,128)(2,1)}, u32[]{:S(2)}) copy-start(bf16[2048,32]{0,1:T(8,128)(2,1)} %param.25) | copy-start | bytes 393220
  1.5 22.9 %copy-start.6 = (bf16[2048,32]{0,1:T(8,128)(2,1)S(1)}, bf16[2048,32]{0,1:T(8,128)(2,1)}, u32[]{:S(2)}) copy-start(bf16[2048,32]{0,1:T(8,128)(2,1)} %param.24) | copy-start | bytes 393220
  20.1 14.0 %collective-permute-start = (bf16[128,2048]{1,0:T(8,128)(2,1)S(1)}, bf16[128,2048]{1,0:T(8,128)(2,1)S(1)}, u32[]{:S(2)}, u32[]{:S(2)}) collective-permute-start(bf16[128,2048]{1,0:T(8,128)(2,1)S(1)} %fusion.5), channel_id=1, source_target_pairs={{0,1},{1,0},{2,3},{3,2},{4,5},{5,4},{6,7},{7,6},{8,9},{9,8},{10,11... | collective-permute-start | bytes 1572872 | tf_op jit(solution)/shard_map/ppermute | solution.py:439
  24.6 10.6 %copy-start.16 = (bf16[2048,1024]{1,0:T(8,128)(2,1)S(1)}, bf16[2048,1024]{1,0:T(8,128)(2,1)}, u32[]{:S(2)}) copy-start(bf16[2048,1024]{1,0:T(8,128)(2,1)} %param.22) | copy-start | bytes 12582916
  35.1 2.2 %copy-start.17 = (bf16[2048,1024]{1,0:T(8,128)(2,1)S(1)}, bf16[2048,1024]{1,0:T(8,128)(2,1)}, u32[]{:S(2)}) copy-start(bf16[2048,1024]{1,0:T(8,128)(2,1)} %param.23) | copy-start | bytes 12582916
  37.3 1.6 copy-start.10
  38.7 19.7 %copy-start.11 = (bf16[272,1024]{1,0:T(8,128)(2,1)}, bf16[272,1024]{1,0:T(8,128)(2,1)S(1)}, u32[]{:S(2)}) copy-start(bf16[272,1024]{1,0:T(8,128)(2,1)S(1)} %convolution_convert_fusion.1.v_ref) | copy-start | bytes 1671172
  54.1 4.3 %copy-start.9 = (f32[256,32]{0,1:T(8,128)S(1)}, f32[256,32]{0,1:T(8,128)}, u32[]{:S(2)}) copy-start(f32[256,32]{0,1:T(8,128)} %param.29) | copy-start | bytes 98308
  59.0 3.4 %copy-start.4 = (f32[256,8,2]{0,2,1:T(2,128)}, f32[256,8,2]{0,2,1:T(2,128)S(1)}, u32[]{:S(2)}) copy-start(f32[256,8,2]{0,2,1:T(2,128)S(1)} %reshape.122) | copy-start | bytes 49156
  61.4 26.9 %copy-start.12 = (f32[1,256]{1,0:T(1,128)}, f32[1,256]{1,0:T(1,128)S(1)}, u32[]{:S(2)}) copy-start(f32[1,256]{1,0:T(1,128)S(1)} %fusion.11) | copy-start | bytes 3076
  142.2 16.6 %copy-start.2 = (bf16[256,1024]{1,0:T(8,128)(2,1)S(1)}, bf16[256,1024]{1,0:T(8,128)(2,1)}, u32[]{:S(2)}) copy-start(bf16[256,1024]{1,0:T(8,128)(2,1)} %read_out.1) | copy-start | bytes 1572868
  145.3 13.6 %collective-permute-start.1 = (bf16[128,2048]{1,0:T(8,128)(2,1)S(1)}, bf16[128,2048]{1,0:T(8,128)(2,1)S(1)}, u32[]{:S(2)}, u32[]{:S(2)}) collective-permute-start(bf16[128,2048]{1,0:T(8,128)(2,1)S(1)} %convolution_convert_fusion), channel_id=1, source_target_pairs={{0,1},{1,0},{2,3},{3,2},{4,5},{5,4},{6,7},{7,6},{8,9},{9,8},{10,11... | collective-permute-start | bytes 1572872 | tf_op jit(solution)/shard_map/ppermute | solution.py:454
